TPU v7x, 32 devices: a whole 2x2x4 slice. The times are simulated.
32 devices in a mesh: tp: 32 (over z, y, x, core).
Axes of the slice: x: 2, y: 2, z: 4, core: 2. Of those that a mesh axis runs over, the one named last changes fastest.
Arguments:
- stream: bfloat16 [1024, 2048], P('tp'), may hold values from -15 to 15
- norm_gain: bfloat16 [4096], replicated, may hold values from 0.099609375 to 1.8984375
- query_weight: bfloat16 [65536, 128], P('tp'), may hold values from -0.09375 to 0.09375
- key_weight: bfloat16 [65536, 128], P('tp'), may hold values from -0.09375 to 0.09375
- value_weight: bfloat16 [65536, 128], P('tp'), may hold values from -0.09375 to 0.09375
- gate_weight: bfloat16 [65536, 128], P('tp'), may hold values from -0.09375 to 0.09375
- write_weight: bfloat16 [4096, 16], replicated, may hold values from -0.09375 to 0.09375
- decay_weight: bfloat16 [4096, 16], replicated, may hold values from -0.09375 to 0.09375
- decay_rate: float32 [16], replicated, may hold values from 0.02 to 2
- head_gain: bfloat16 [128], replicated, may hold values from 0.099609375 to 1.8984375
- out_weight: bfloat16 [65536, 128], P('tp'), may hold values from -0.125 to 0.125
- state: float32 [8192, 128, 128], P('tp'), may hold values from -4 to 4
Outputs:
- stream_out: bfloat16 [1024, 2048], P('tp')
- state_out: float32 [8192, 128, 128], P('tp')
All inputs are finite; a program needn't handle non-finite values.
Results may differ from a plain program's by a relative error of at most 0.012.
Values may be sent and summed in bfloat16 or wider, within the bound.
A program may use at most 128 MiB of HBM per device.

v0:
```python
import functools

import jax
import jax.numpy as jnp
from jax import lax
from jax.experimental import pallas as pl
from jax.experimental.pallas import tpu as pltpu
from jax.sharding import PartitionSpec as P

EPS = 1e-06
MESH = pl.DeviceIdType.MESH
VMEM = pl.BlockSpec(memory_space=pltpu.VMEM)
SMALL = 16


def flip(me, bits):
    other = me
    for bit in bits:
        other = other + (1 - 2 * ((me // (1 << bit)) % 2)) * (1 << bit)
    return other


def parts_of(cols, dims):
    tiles = cols // 128
    count = max(1, min(dims, tiles))
    cuts = [tiles * i // count * 128 for i in range(count + 1)]
    ranges = [(cuts[i], cuts[i + 1] - cuts[i]) for i in range(count)]
    orders = [[1 + (i + j) % dims for j in range(dims)] for i in range(count)]
    return list(zip(ranges, orders))


def masks_of(order):
    sets = [((), -1)]
    for step in range(len(order)):
        sets = sets + [(bits + (order[step],), step) for bits, _ in sets]
    return sets


def key_of(bits):
    return sum(1 << (bit - 1) for bit in bits)


def enter(devices):
    barrier = pltpu.get_barrier_semaphore()
    for device in devices:
        pl.semaphore_signal(barrier, inc=1, device_id=(device,), device_id_type=MESH)
    pl.semaphore_wait(barrier, len(devices))


def remote(source, target, send_sem, recv_sem, device):
    return pltpu.make_async_remote_copy(
        src_ref=source,
        dst_ref=target,
        send_sem=send_sem,
        recv_sem=recv_sem,
        device_id=(device,),
        device_id_type=MESH,
    )


def project_kernel(
    heads,
    groups,
    stream_ref,
    gain_ref,
    query_w,
    key_w,
    value_w,
    gate_w,
    write_w,
    decay_w,
    rate_ref,
    packed_out,
    gathered,
    weights,
    write_t,
    decay_t,
    gains,
    local_sems,
    partial,
    sent,
    received,
    small_sent,
    small_received,
    turned,
    ici_send,
    ici_recv,
    core_send,
    core_recv,
    group_send,
    group_recv,
    small_send,
    small_recv,
):
    me = lax.axis_index("tp")
    place = me % heads
    group = me // heads
    rows, cols = stream_ref.shape
    batch = gathered.shape[0]
    group_rows = batch // groups
    dims = heads.bit_length() - 2
    sibling = flip(me, (0,))
    neighbours = [flip(me, (bit,)) for bit in range(1, dims + 1)]
    others = [place + heads * ((group + j) % groups) for j in range(1, groups)]
    size = query_w.shape[1]
    own_cols = pl.ds(pl.multiple_of(group * cols, cols), cols)
    fetches = [
        pltpu.make_async_copy(
            weight, weights.at[:, i * size : (i + 1) * size], local_sems.at[i]
        )
        for i, weight in enumerate((query_w, key_w, value_w, gate_w))
    ] + [
        pltpu.make_async_copy(source.at[:, own_cols], target, local_sems.at[4 + i])
        for i, (source, target) in enumerate(((write_w, write_t), (decay_w, decay_t)))
    ]
    for fetch in fetches:
        fetch.start()
    enter([sibling] + neighbours + others)

    halves = 2 if rows % 32 == 0 and group_rows % rows == 0 else 1
    part_rows = rows // halves
    half_batch = batch // halves
    ranges = parts_of(cols, dims)

    def half_rows(h, device_place):
        begin = h * half_batch + device_place * part_rows
        return pl.ds(pl.multiple_of(begin, part_rows), part_rows)

    def block(h, device_place, part):
        return gathered.at[half_rows(h, device_place), pl.ds(part[0][0], part[0][1])]

    sends = []
    core_copies = [[] for _ in range(halves)]

    def pass_on(h, p, part, bits, step):
        order = part[1]
        origin = flip(place, bits)
        target = block(h, origin, part)
        if bits:
            source = target
        else:
            source = stream_ref.at[
                pl.ds(h * part_rows, part_rows), pl.ds(part[0][0], part[0][1])
            ]
        for later in range(step + 1, dims):
            landed = key_of(bits + (order[later],))
            copy = remote(
                source,
                target,
                ici_send.at[h, p, landed],
                ici_recv.at[h, p, landed],
                flip(me, (order[later],)),
            )
            copy.start()
            sends.append(copy)
        own = key_of(bits)
        copy = remote(source, target, core_send.at[h, p, own], core_recv.at[h, p, own], sibling)
        copy.start()
        core_copies[h].append(copy)

    def begin(h):
        for p, part in enumerate(ranges):
            pass_on(h, p, part, (), -1)

    def relay(h, index):
        for p, part in enumerate(ranges):
            bits, step = masks_of(part[1])[index]
            landed = key_of(bits)
            target = block(h, flip(place, bits), part)
            remote(
                target, target, ici_send.at[h, p, landed], ici_recv.at[h, p, landed], sibling
            ).wait_recv()
            pass_on(h, p, part, bits, step)

    early = max(2, 1 << (dims - 1))
    begin(0)
    for h in range(halves):
        gathered[half_rows(h, place), :] = stream_ref[h * part_rows : (h + 1) * part_rows, :]
    relay(0, 1)
    for h in range(1, halves):
        begin(h)
    for index in range(2, 1 << dims):
        relay(0, index)
    for h in range(1, halves):
        for index in range(1, early):
            relay(h, index)
    for copy in core_copies[0]:
        copy.wait_recv()

    gains[...] = gain_ref[...].astype(jnp.float32)
    gain = jnp.concatenate(
        [gains[pl.ds(group * (cols // 128) + i, 1), :] for i in range(cols // 128)], axis=1
    )
    for fetch in fetches:
        fetch.wait()

    def project(begin, count, at):
        x = gathered[pl.ds(begin, count), :].astype(jnp.float32)
        gained = (x * gain).astype(jnp.bfloat16)
        partial[pl.ds(at, count), :] = jnp.dot(
            gained, weights[...], preferred_element_type=jnp.float32
        )
        mine = lax.broadcasted_iota(jnp.int32, (count, heads), 1) == place
        pre = [
            jnp.sum(
                jnp.where(
                    mine,
                    lax.dot_general(
                        gained,
                        w[...],
                        (((1,), (1,)), ((), ())),
                        preferred_element_type=jnp.float32,
                    ),
                    0.0,
                ),
                axis=1,
                keepdims=True,
            )
            for w in (write_t, decay_t)
        ]
        squares = jnp.sum(x * x, axis=1, keepdims=True)
        lane = lax.broadcasted_iota(jnp.int32, (count, 128), 1)
        return jnp.where(
            lane == 0, pre[0], jnp.where(lane == 1, pre[1], jnp.where(lane == 2, squares, 0.0))
        )

    copies = []
    wide = max(group_rows, 128)
    count = group_rows // halves

    def half_of(h, target_group):
        begin = h * half_batch + target_group * count
        return pl.multiple_of(begin, count)

    for h in range(halves):
        if h:
            for index in range(early, 1 << dims):
                relay(h, index)
            for copy in core_copies[h]:
                copy.wait_recv()
        for j in range(1, groups):
            spot = slice(h * count, (h + 1) * count)
            side = project(half_of(h, (group + j) % groups), count, 0)
            sent[j - 1, spot] = partial[0:count].astype(jnp.bfloat16)
            turned[spot] = side
            routes = [(sent.at[j - 1, spot], received.at[j - 1, spot], group_send, group_recv)]
            flat = turned[...].T
            small_sent[j - 1, :, spot] = flat[0:SMALL, spot].astype(jnp.bfloat16)
            routes.append(
                (
                    small_sent.at[j - 1, :, spot],
                    small_received.at[j - 1, :, spot],
                    small_send,
                    small_recv,
                )
            )
            for source, target, send, recv in routes:
                copy = remote(
                    source, target, send.at[h, j - 1], recv.at[h, j - 1], others[j - 1]
                )
                copy.start()
                copies.append(copy)
    for h in range(halves):
        turned[h * count : (h + 1) * count] = project(half_of(h, group), count, h * count)
    total = partial[...]
    flat = turned[...].T[0:SMALL, :]
    for copy in copies:
        copy.wait_recv()
    for j in range(1, groups):
        total = total + received[j - 1].astype(jnp.float32)
    small_total = flat[:, 0:group_rows]
    for j in range(1, groups):
        small_total = small_total + small_received[j - 1].astype(jnp.float32)
    turned_back = jnp.concatenate(
        [small_total, jnp.zeros((SMALL, wide - group_rows), jnp.float32)], axis=1
    ) if wide > group_rows else small_total
    side = jnp.concatenate(
        [turned_back, jnp.zeros((128 - SMALL, wide), jnp.float32)], axis=0
    ).T[0:group_rows]
    scale = lax.rsqrt(side[:, 2:3] / (cols * groups) + EPS)

    def rounded(v):
        return v.astype(jnp.bfloat16).astype(jnp.float32)

    projected = rounded(total * scale)
    query = projected[:, :size]
    key = projected[:, size : 2 * size]
    query = query * lax.rsqrt(jnp.sum(query * query, axis=1, keepdims=True) + EPS) * size**-0.5
    key = key * lax.rsqrt(jnp.sum(key * key, axis=1, keepdims=True) + EPS)
    pre = rounded(side * scale)
    strength = jax.nn.sigmoid(pre[:, 0:1])
    mine = lax.broadcasted_iota(jnp.int32, rate_ref.shape, 1) == place
    rate = jnp.sum(jnp.where(mine, rate_ref[...], 0.0), axis=1, keepdims=True)
    decay = pre[:, 1:2]
    softplus = jnp.maximum(decay, 0.0) + jnp.log(1.0 + jnp.exp(-jnp.abs(decay)))
    factor = jnp.exp(-rate * softplus)
    overlap = jnp.sum(query * key, axis=1, keepdims=True)
    results = [jnp.broadcast_to(v, (group_rows, size)) for v in (strength, factor, overlap)]
    results += [query, key, projected[:, 2 * size :]]
    for i, v in enumerate(results):
        span = pl.ds(i * size, v.shape[1])
        if halves == 1:
            packed_out[:, span] = v
            continue
        for h in range(halves):
            for q in range(group_rows // rows):
                to, come = q * rows + h * part_rows, h * count + q * part_rows
                packed_out[to : to + part_rows, span] = v[come : come + part_rows]
    for copy in sends + sum(core_copies, []) + copies:
        copy.wait_send()


def project(stream, norm_gain, weights, write_weight, decay_weight, rate, heads, groups):
    rows, cols = stream.shape
    batch = rows * heads
    group_rows = batch // groups
    size = weights[0].shape[1]
    dims = heads.bit_length() - 2
    parts = len(parts_of(cols, dims))
    extra = groups - 1
    halves = 2
    dma = pltpu.SemaphoreType.DMA
    anywhere = pl.BlockSpec(memory_space=pl.ANY)
    return pl.pallas_call(
        functools.partial(project_kernel, heads, groups),
        in_specs=[VMEM] * 2 + [anywhere] * 6 + [VMEM],
        out_specs=VMEM,
        out_shape=jax.ShapeDtypeStruct((group_rows, 7 * size), jnp.float32),
        scratch_shapes=[
            pltpu.VMEM((batch, cols), jnp.bfloat16),
            pltpu.VMEM((cols, 4 * size), jnp.bfloat16),
            pltpu.VMEM((heads, cols), jnp.bfloat16),
            pltpu.VMEM((heads, cols), jnp.bfloat16),
            pltpu.VMEM((groups * cols // 128, 128), jnp.float32),
            dma((6,)),
            pltpu.VMEM((group_rows, 4 * size), jnp.float32),
            pltpu.VMEM((extra, group_rows, 4 * size), jnp.bfloat16),
            pltpu.VMEM((extra, group_rows, 4 * size), jnp.bfloat16),
            pltpu.VMEM((extra, SMALL, group_rows), jnp.bfloat16),
            pltpu.VMEM((extra, SMALL, group_rows), jnp.bfloat16),
            pltpu.VMEM((max(group_rows, 128), 128), jnp.float32),
            dma((halves, parts, 1 << dims)),
            dma((halves, parts, 1 << dims)),
            dma((halves, parts, 1 << dims)),
            dma((halves, parts, 1 << dims)),
            dma((halves, extra)),
            dma((halves, extra)),
            dma((halves, extra)),
            dma((halves, extra)),
        ],
        compiler_params=pltpu.CompilerParams(
            collective_id=0, has_side_effects=True
        ),
    )(
        stream,
        norm_gain.reshape(groups * cols // 128, 128),
        *weights,
        write_weight.T,
        decay_weight.T,
        rate.reshape(1, heads),
    )


def split(v):
    high = v.astype(jnp.bfloat16)
    return high, (v - high.astype(jnp.float32)).astype(jnp.bfloat16)


def state_kernel(
    state_ref, packed_ref, gain_ref, new_ref, gated_ref, flat_ref, held, readout, in_sems, out_sems
):
    total, size, _ = state_ref.shape
    steps = in_sems.shape[0]
    count = total // steps

    def rows_of(step):
        return pl.ds(pl.multiple_of(step * count, count), count)

    def fetch(step):
        rows = rows_of(step)
        return pltpu.make_async_copy(state_ref.at[rows], held.at[rows], in_sems.at[step])

    def store(step):
        rows = rows_of(step)
        return pltpu.make_async_copy(held.at[rows], new_ref.at[rows], out_sems.at[step])

    for step in range(steps):
        fetch(step).start()
    spots = lax.broadcasted_iota(jnp.int32, (4 * count, size), 0) % count

    def diagonal(rows):
        marks = spots[0 : rows.shape[0]]
        return jnp.concatenate(
            [jnp.where(marks == b, rows, jnp.zeros_like(rows)) for b in range(count)], axis=1
        )

    def body(step, carry):
        rows = rows_of(step)

        def columns(first, width=1):
            return packed_ref[rows, first * size : (first + width) * size]

        key_high, key_low = split(columns(4))
        query_high, query_low = split(columns(3))
        four = jnp.concatenate([key_high, key_low, query_high, query_low], axis=0)
        strength, factor, overlap = columns(0), columns(1), columns(2)
        left = jnp.concatenate([key_high, key_low, key_high], axis=0)
        left = jnp.concatenate([left, jnp.zeros((size - 3 * count, size), left.dtype)], axis=0)
        left = left.astype(jnp.float32).T.astype(jnp.bfloat16)[:, 0 : 3 * count]
        wide = diagonal(four)
        fetch(step).wait()
        memory = held[rows].reshape(count * size, size).astype(jnp.bfloat16)
        both = jnp.dot(wide, memory, preferred_element_type=jnp.float32)
        recalled = both[0:count] + both[count : 2 * count]
        asked = both[2 * count : 3 * count] + both[3 * count : 4 * count]
        change = strength * (columns(5) - factor * recalled)
        readout[rows, :] = factor * asked + overlap * change
        change_high, change_low = split(change)
        right = diagonal(jnp.concatenate([change_high, change_high, change_low], axis=0))
        outer = jnp.dot(left, right, preferred_element_type=jnp.float32)
        for b in range(count):
            spot = step * count + b
            held[spot] = factor[b : b + 1, :] * held[spot] + outer[:, b * size : (b + 1) * size]
        store(step).start()
        return carry

    lax.fori_loop(0, steps, body, 0)
    read = readout[...]
    scaling = lax.rsqrt(jnp.sum(read * read, axis=1, keepdims=True) / size + EPS)
    gate = packed_ref[:, 6 * size :]
    gated_ref[...] = (
        read * gain_ref[...].astype(jnp.float32) * (gate / (1.0 + jnp.exp(-gate)))
    ).astype(jnp.bfloat16)
    tall = jnp.broadcast_to(scaling, (total, 128))
    if total < 128:
        tall = jnp.concatenate([tall, jnp.zeros((128 - total, 128), jnp.float32)], axis=0)
    flat_ref[...] = tall.T[0:SMALL, 0:total].astype(jnp.bfloat16)
    for step in range(steps):
        store(step).wait()


def state_step(state, packed, head_gain):
    count, size, _ = state.shape
    steps = count // min(16, count)
    anywhere = pl.BlockSpec(memory_space=pl.ANY)
    return pl.pallas_call(
        state_kernel,
        in_specs=[anywhere, VMEM, VMEM],
        out_specs=[anywhere, VMEM, VMEM],
        out_shape=[
            jax.ShapeDtypeStruct(state.shape, state.dtype),
            jax.ShapeDtypeStruct((count, size), jnp.bfloat16),
            jax.ShapeDtypeStruct((SMALL, count), jnp.bfloat16),
        ],
        scratch_shapes=[
            pltpu.VMEM(state.shape, state.dtype),
            pltpu.VMEM((count, size), jnp.float32),
            pltpu.SemaphoreType.DMA((steps,)),
            pltpu.SemaphoreType.DMA((steps,)),
        ],
    )(state, packed, head_gain.reshape(1, size))


def output_kernel(
    heads,
    groups,
    stream_ref,
    gated_ref,
    scaling_ref,
    weight_hbm,
    out_ref,
    weight_ref,
    weight_sem,
    all_gated,
    all_scaling,
    columns,
    held,
    core_out,
    core_in,
    hop_out,
    hop_in,
    gated_send,
    gated_recv,
    scaling_send,
    scaling_recv,
    core_send,
    core_recv,
    hop_send,
    hop_recv,
):
    me = lax.axis_index("tp")
    place = me % heads
    group = me // heads
    rows, cols = stream_ref.shape
    batch = all_gated.shape[0]
    group_rows = batch // groups
    dims = heads.bit_length() - 2
    chips = 1 << dims
    sibling = flip(me, (0,))
    neighbours = [flip(me, (bit,)) for bit in range(1, dims + 1)]
    others = [place + heads * ((group + j) % groups) for j in range(1, groups)]
    weight_copy = pltpu.make_async_copy(weight_hbm, weight_ref, weight_sem)
    weight_copy.start()
    enter([sibling] + neighbours + others)
    own_rows = pl.ds(pl.multiple_of(group * group_rows, group_rows), group_rows)
    copies = []
    arriving = []
    for j in range(1, groups):
        for source, target, send, recv in (
            (gated_ref, all_gated.at[own_rows], gated_send, gated_recv),
            (scaling_ref, all_scaling.at[group], scaling_send, scaling_recv),
        ):
            copy = remote(source, target, send.at[j - 1], recv.at[j - 1], others[j - 1])
            copy.start()
            copies.append(copy)
    all_gated[own_rows, :] = gated_ref[...]
    all_scaling[group] = scaling_ref[...]
    for copy in copies:
        copy.wait_recv()
    weight_copy.wait()
    wide = max(group_rows, 128)
    for g in range(groups):
        flat = all_scaling[g].astype(jnp.float32)
        if wide > group_rows:
            flat = jnp.concatenate(
                [flat, jnp.zeros((SMALL, wide - group_rows), jnp.float32)], axis=1
            )
        flat = jnp.concatenate([flat, jnp.zeros((128 - SMALL, wide), jnp.float32)], axis=0)
        columns[g * group_rows : (g + 1) * group_rows, :] = flat.T[0:group_rows]

    def relative(owner, mask):
        bits = tuple(bit for bit in range(1, dims + 1) if mask >> (bit - 1) & 1)
        begin = flip(owner, bits) * rows
        return pl.ds(pl.multiple_of(begin, rows), rows)

    def head_rows(owner, masks):
        picks = [relative(owner, mask) for mask in masks]
        left = jnp.concatenate([all_gated[pick, :] for pick in picks], axis=0)
        scale = jnp.concatenate([columns[pick, 0:1] for pick in picks], axis=0)
        product = lax.dot_general(
            left, weight_ref[...], (((1,), (1,)), ((), ())), preferred_element_type=jnp.float32
        )
        return product * scale

    core_copies = [
        remote(
            core_out.at[mask], core_in.at[mask], core_send.at[mask], core_recv.at[mask], sibling
        )
        for mask in range(chips)
    ]
    batch_of = min(4, chips)
    sweep = list(range(chips - 1, -1, -1))
    for first in range(0, chips, batch_of):
        masks = sweep[first : first + batch_of]
        product = head_rows(flip(place, (0,)), masks).astype(jnp.bfloat16)
        for i, mask in enumerate(masks):
            core_out[mask] = product[i * rows : (i + 1) * rows]
            core_copies[mask].start()
    for first in range(0, chips, batch_of):
        masks = sweep[first : first + batch_of]
        product = head_rows(place, masks)
        for i, mask in enumerate(masks):
            held[mask] = product[i * rows : (i + 1) * rows]

    parts = parts_of(cols, dims)
    hops = []
    waiting = [[] for _ in range(dims)]

    def cross(step, p, mask):
        (start, width), order = parts[p]
        if step == dims or not mask >> (order[step] - 1) & 1:
            return
        span = pl.ds(start, width)
        landed = mask - (1 << (order[step] - 1))
        hop_out[step, landed, :, span] = held[mask, :, span].astype(jnp.bfloat16)
        copy = remote(
            hop_out.at[step, landed, :, span],
            hop_in.at[step, landed, :, span],
            hop_send.at[step, p, landed],
            hop_recv.at[step, p, landed],
            neighbours[order[step] - 1],
        )
        copy.start()
        hops.append(copy)
        waiting[step].append((p, landed, span, copy))

    for mask in sweep:
        core_copies[mask].wait_recv()
        held[mask] += core_in[mask].astype(jnp.float32)
        for p in range(len(parts)):
            cross(0, p, mask)
    for step in range(dims):
        for p, landed, span, copy in waiting[step]:
            copy.wait_recv()
            held[landed, :, span] += hop_in[step, landed, :, span].astype(jnp.float32)
            cross(step + 1, p, landed)
    out_ref[...] = (stream_ref[...].astype(jnp.float32) + held[0]).astype(jnp.bfloat16)
    for copy in copies + core_copies + hops:
        copy.wait_send()


def output(stream, gated, scaling, out_weight, heads, groups):
    rows, cols = stream.shape
    batch = rows * heads
    group_rows, size = gated.shape
    dims = heads.bit_length() - 2
    chips = 1 << dims
    parts = len(parts_of(cols, dims))
    extra = groups - 1
    dma = pltpu.SemaphoreType.DMA
    anywhere = pl.BlockSpec(memory_space=pl.ANY)
    return pl.pallas_call(
        functools.partial(output_kernel, heads, groups),
        in_specs=[VMEM] * 3 + [anywhere],
        out_specs=VMEM,
        out_shape=jax.ShapeDtypeStruct(stream.shape, stream.dtype),
        scratch_shapes=[
            pltpu.VMEM(out_weight.shape, out_weight.dtype),
            dma(()),
            pltpu.VMEM((batch, size), jnp.bfloat16),
            pltpu.VMEM((groups, SMALL, group_rows), jnp.bfloat16),
            pltpu.VMEM((batch, 128), jnp.float32),
            pltpu.VMEM((chips, rows, cols), jnp.float32),
            pltpu.VMEM((chips, rows, cols), jnp.bfloat16),
            pltpu.VMEM((chips, rows, cols), jnp.bfloat16),
            pltpu.VMEM((dims, chips, rows, cols), jnp.bfloat16),
            pltpu.VMEM((dims, chips, rows, cols), jnp.bfloat16),
            dma((extra,)),
            dma((extra,)),
            dma((extra,)),
            dma((extra,)),
            dma((chips,)),
            dma((chips,)),
            dma((dims, parts, chips)),
            dma((dims, parts, chips)),
        ],
        compiler_params=pltpu.CompilerParams(
            collective_id=1, has_side_effects=True
        ),
    )(stream, gated, scaling, out_weight)


def per_device(
    stream,
    norm_gain,
    query_weight,
    key_weight,
    value_weight,
    gate_weight,
    write_weight,
    decay_weight,
    decay_rate,
    head_gain,
    out_weight,
    state,
):
    heads = decay_rate.shape[0]
    groups = lax.axis_size("tp") // heads
    weights = (query_weight, key_weight, value_weight, gate_weight)
    packed = project(
        stream, norm_gain, weights, write_weight, decay_weight, decay_rate, heads, groups
    )
    updated, gated, scaling = state_step(state, packed, head_gain)
    result = output(stream, gated, scaling, out_weight, heads, groups)
    return (result, updated)


def solution(mesh):
    placed = (
        P("tp", None),
        P(),
        P("tp", None),
        P("tp", None),
        P("tp", None),
        P("tp", None),
        P(),
        P(),
        P(),
        P(),
        P("tp", None),
        P("tp", None, None),
    )
    return jax.shard_map(
        per_device,
        mesh=mesh,
        in_specs=placed,
        out_specs=(P("tp", None), P("tp", None, None)),
        check_vma=False,
    )
```

profile of v0, /device:TPU:0, one launch (start us, length us, event | category | flops | bytes accessed | tf_op | source)
XLA Modules:
  0.0 72.0 jit_solution(2765257124837227131)
XLA Ops:
  0.6 34.4 %shard_map.131.packed_ref = f32[256,896]{1,0:T(8,128)} custom-call(bf16[32,2048]{1,0:T(8,128)(2,1)} %stream_ref.3, bf16[32,128]{1,0:T(8,128)(2,1)} %bitcast.7, bf16[2048,128]{1,0:T(8,128)(2,1)} %query_w.1, bf16[2048,128]{1,0:T(8,128)(2,1)} %key_w.1, bf16[2048,128]{1,0:T(8,128)(2,1)} %value_w.1, bf16[2048,128]{1,0:T(8,128)(2,1)} %gate_w.1, ...), custom_call_target="tpu_custom_call" | custom-call | tf_op jit(solution)/shard_map/pallas_call | solution.py:324
  35.0 14.1 %shard_map.132 = (f32[256,128,128]{2,1,0:T(8,128)}, bf16[256,128]{1,0:T(8,128)(2,1)}, bf16[16,256]{1,0:T(8,128)(2,1)}) custom-call(f32[256,128,128]{2,1,0:T(8,128)} %state_ref.1, f32[256,896]{1,0:T(8,128)} %shard_map.131.packed_ref, bf16[1,128]{1,0:T(2,128)(2,1)} %bitcast.8), custom_call_target="tpu_custom_call" | custom-call | tf_op jit(solution)/shard_map/pallas_call | solution.py:446
  49.1 21.3 %shard_map.133 = bf16[32,2048]{1,0:T(8,128)(2,1)} custom-call(bf16[32,2048]{1,0:T(8,128)(2,1)} %stream_ref.3, bf16[256,128]{1,0:T(8,128)(2,1)} %get-tuple-element.5.gated_ref, bf16[16,256]{1,0:T(8,128)(2,1)} %get-tuple-element.6.scaling_ref, bf16[2048,128]{1,0:T(8,128)(2,1)} %weight_hbm.1), custom_call_target="tpu_custom_call" | custom-call | tf_op jit(solution)/shard_map/pallas_call | solution.py:612
  70.4 1.6 %copy.15 = bf16[32,2048]{1,0:T(8,128)(2,1)} copy(bf16[32,2048]{1,0:T(8,128)(2,1)} %shard_map.133) | data formatting | bytes 262144
where the time goes:
time: 72.2 us; the launch traced here: 72 us
  Pallas kernels  69.8 us (97%)
  local copies, waits for them, and re-layouts  1.57 us (2%)
    pallas_call x1, Pallas kernels, project(): pl.pallas_call(functools.partial(project_kernel, heads, groups), in_specs...  34.4 us
    pallas_call x1, Pallas kernels, output(): pl.pallas_call(functools.partial(output_kernel, heads, groups), in_specs=...  21.3 us
    pallas_call x1, Pallas kernels, state_step(): pl.pallas_call(state_kernel, in_specs=[anywhere, VMEM, VMEM], out_specs=[...  14.1 us
    unnamed x1, local copies, waits for them, and re-layouts  1.57 us

commit v1 on v0

--- a/solution.py
+++ b/solution.py
@@ -640,6 +640,581 @@
     )(stream, gated, scaling, out_weight)
 
 
+def masked(mask, dims):
+    return tuple(bit for bit in range(1, dims + 1) if mask >> (bit - 1) & 1)
+
+
+def fused_kernel(
+    heads,
+    groups,
+    stream_ref,
+    gain_ref,
+    query_w,
+    key_w,
+    value_w,
+    gate_w,
+    write_w,
+    decay_w,
+    rate_ref,
+    head_gain_ref,
+    out_w,
+    state_ref,
+    held,
+    packed,
+    result,
+    gathered,
+    weights,
+    side_w,
+    gain_row,
+    gains,
+    both_w,
+    partial,
+    partial_side,
+    sent,
+    received,
+    small_sent,
+    small_received,
+    work,
+    gated,
+    left,
+    acc,
+    hop_out,
+    hop_in,
+    last_out,
+    last_in,
+    up_out,
+    up_in,
+    local_sems,
+    state_sems,
+    pair_sems,
+    ici_send,
+    ici_recv,
+    core_send,
+    core_recv,
+    main_send,
+    main_recv,
+    small_send,
+    small_recv,
+    gated_send,
+    gated_recv,
+    hop_send,
+    hop_recv,
+    last_send,
+    last_recv,
+    up_send,
+    up_recv,
+):
+    me = lax.axis_index("tp")
+    place = me % heads
+    group = me // heads
+    core = place % 2
+    rows, cols = stream_ref.shape
+    size = query_w.shape[1]
+    dims = heads.bit_length() - 2
+    chips = 1 << dims
+    flats = chips // 2
+    chip_rows = 2 * rows
+    count = held.shape[0] // state_sems.shape[0]
+    sibling = flip(me, (0,))
+    neighbours = [flip(me, (bit,)) for bit in range(1, dims + 1)]
+    partner = place + heads * ((group + 1) % groups)
+    partner_sibling = flip(partner, (0,))
+    own_cols = pl.ds(pl.multiple_of(group * cols, cols), cols)
+    upper = place // flats // 2
+    keep = (upper + group) % 2
+
+    fetches = [
+        pltpu.make_async_copy(
+            weight, weights.at[:, i * size : (i + 1) * size], local_sems.at[i]
+        )
+        for i, weight in enumerate((query_w, key_w, value_w, gate_w))
+    ] + [
+        pltpu.make_async_copy(
+            source.at[:, own_cols], side_w.at[i * heads : (i + 1) * heads], local_sems.at[4 + i]
+        )
+        for i, source in enumerate((write_w, decay_w))
+    ]
+    own_half = pltpu.make_async_copy(out_w, both_w.at[:, 0:size], local_sems.at[6])
+    other_half = remote(
+        out_w, both_w.at[:, size : 2 * size], pair_sems.at[0], pair_sems.at[1], sibling
+    )
+
+    def fetch(step):
+        spot = pl.ds(pl.multiple_of(step * count, count), count)
+        return pltpu.make_async_copy(state_ref.at[spot], held.at[spot], state_sems.at[step])
+
+    for copy in fetches:
+        copy.start()
+    enter([sibling] + neighbours + [partner, partner_sibling])
+
+    half = rows // 2
+    top = dims
+    parts = [(0, (top, 1, 2)), (half, (top, 2, 1))]
+
+    def block(device_place, p):
+        begin = device_place * rows + parts[p][0]
+        return gathered.at[pl.ds(pl.multiple_of(begin, half), half), :]
+
+    sends = []
+
+    def pass_on(p, bits):
+        order = parts[p][1]
+        step = max([order.index(bit) for bit in bits], default=-1)
+        target = block(flip(place, bits), p)
+        source = target if bits else stream_ref.at[parts[p][0] : parts[p][0] + half, :]
+        for later in range(step + 1, dims):
+            landed = key_of(bits + (order[later],))
+            copy = remote(
+                source,
+                target,
+                ici_send.at[p, landed],
+                ici_recv.at[p, landed],
+                flip(me, (order[later],)),
+            )
+            copy.start()
+            sends.append(copy)
+        own = key_of(bits)
+        copy = remote(source, target, core_send.at[p, own], core_recv.at[p, own], sibling)
+        copy.start()
+        sends.append(copy)
+
+    def relay(p, mask):
+        bits = masked(mask, dims)
+        target = block(flip(place, bits), p)
+        remote(target, target, ici_send.at[p, mask], ici_recv.at[p, mask], sibling).wait_recv()
+        pass_on(p, bits)
+
+    def from_sibling(mask):
+        for p in range(2):
+            target = block(flip(sibling % heads, masked(mask, dims)), p)
+            remote(
+                target, target, core_send.at[p, mask], core_recv.at[p, mask], sibling
+            ).wait_recv()
+
+    for p in range(2):
+        pass_on(p, ())
+    gathered[pl.ds(pl.multiple_of(place * rows, rows), rows), :] = stream_ref[...]
+    gains[...] = gain_ref[...].astype(jnp.float32)
+    tiles = cols // 128
+    for i in range(tiles):
+        gain_row[:, i * 128 : (i + 1) * 128] = gains[pl.ds(group * tiles + i, 1), :]
+    for copy in fetches:
+        copy.wait()
+    for step in range(state_sems.shape[0]):
+        fetch(step).start()
+    own_half.start()
+
+    main_copies = [
+        remote(sent.at[c], received.at[c], main_send.at[c], main_recv.at[c], partner)
+        for c in range(flats)
+    ]
+    small_copies = [
+        remote(
+            small_sent.at[c], small_received.at[c], small_send.at[c], small_recv.at[c], partner
+        )
+        for c in range(flats)
+    ]
+
+    def project(mask):
+        c = mask % flats
+        begin = flip(place, masked(mask, dims)) // 2 * chip_rows
+        from_sibling(mask)
+        x = gathered[pl.ds(pl.multiple_of(begin, chip_rows), chip_rows), :].astype(jnp.float32)
+        gained = (x * gain_row[...]).astype(jnp.bfloat16)
+        product = jnp.dot(gained, weights[...], preferred_element_type=jnp.float32)
+        pre = lax.dot_general(
+            gained, side_w[...], (((1,), (1,)), ((), ())), preferred_element_type=jnp.float32
+        )
+        spot = lax.broadcasted_iota(jnp.int32, pre.shape, 1)
+        write = jnp.sum(jnp.where(spot == place, pre, 0.0), axis=1, keepdims=True)
+        decay = jnp.sum(jnp.where(spot == place + heads, pre, 0.0), axis=1, keepdims=True)
+        squares = jnp.sum(x * x, axis=1, keepdims=True)
+        lane = lax.broadcasted_iota(jnp.int32, (chip_rows, 128), 1)
+        side = jnp.where(
+            lane == 0, write, jnp.where(lane == 1, decay, jnp.where(lane == 2, squares, 0.0))
+        )
+        away = (upper + mask // flats + group) % 2
+
+        @pl.when(away == 1)
+        def _():
+            sent[c] = product.astype(jnp.bfloat16)
+            main_copies[c].start()
+            tall = jnp.concatenate(
+                [side, jnp.zeros((128 - chip_rows, 128), jnp.float32)], axis=0
+            ) if chip_rows < 128 else side
+            small_sent[c] = tall.T[0:SMALL].astype(jnp.bfloat16)
+            small_copies[c].start()
+
+        @pl.when(away == 0)
+        def _():
+            partial[c] = product
+            partial_side[c] = side
+
+    spots = lax.broadcasted_iota(jnp.int32, (4 * count, size), 0) % count
+
+    def diagonal(values):
+        marks = spots[0 : values.shape[0]]
+        return jnp.concatenate(
+            [jnp.where(marks == b, values, jnp.zeros_like(values)) for b in range(count)], axis=1
+        )
+
+    def rounded(v):
+        return v.astype(jnp.bfloat16).astype(jnp.float32)
+
+    mine = lax.broadcasted_iota(jnp.int32, rate_ref.shape, 1) == place
+    rate = jnp.sum(jnp.where(mine, rate_ref[...], 0.0), axis=1, keepdims=True)
+    shares = []
+
+    def recall(c):
+        main_copies[c].wait_recv()
+        small_copies[c].wait_recv()
+        begin = flip(place, masked(c, dims)) // 2 % flats * chip_rows
+        whole = pl.ds(pl.multiple_of(begin, chip_rows), chip_rows)
+        total = partial[c] + received[c].astype(jnp.float32)
+        flat = small_received[c].astype(jnp.float32)
+        flat = jnp.concatenate([flat, jnp.zeros((128 - SMALL, flat.shape[1]), jnp.float32)], axis=0)
+        side = partial_side[c] + flat.T[0:chip_rows]
+        scale = lax.rsqrt(side[:, 2:3] / (cols * groups) + EPS)
+        projected = rounded(total * scale)
+        query = projected[:, :size]
+        key = projected[:, size : 2 * size]
+        query = query * lax.rsqrt(jnp.sum(query * query, axis=1, keepdims=True) + EPS) * size**-0.5
+        key = key * lax.rsqrt(jnp.sum(key * key, axis=1, keepdims=True) + EPS)
+        pre = rounded(side * scale)
+        strength = jax.nn.sigmoid(pre[:, 0:1])
+        decay = pre[:, 1:2]
+        softplus = jnp.maximum(decay, 0.0) + jnp.log(1.0 + jnp.exp(-jnp.abs(decay)))
+        factor = jnp.broadcast_to(jnp.exp(-rate * softplus), (chip_rows, size))
+        overlap = jnp.sum(query * key, axis=1, keepdims=True)
+        gate = projected[:, 3 * size :]
+        lift = head_gain_ref[...].astype(jnp.float32) * (gate / (1.0 + jnp.exp(-gate)))
+        packed[whole, 0:size] = key
+        packed[whole, 2 * size : 3 * size] = factor
+        work[:, 0:size] = query
+        work[:, size : 2 * size] = projected[:, 2 * size : 3 * size]
+        work[:, 2 * size : 3 * size] = lift
+        work[:, 3 * size : 4 * size] = jnp.broadcast_to(strength, (chip_rows, size))
+        work[:, 4 * size : 5 * size] = jnp.broadcast_to(overlap, (chip_rows, size))
+
+        def body(i, carry):
+            near = pl.ds(pl.multiple_of(i * count, count), count)
+            step = begin // count + i
+            spot = pl.ds(pl.multiple_of(begin + i * count, count), count)
+            key_high, key_low = split(packed[spot, 0:size])
+            query_high, query_low = split(work[near, 0:size])
+            wide = diagonal(jnp.concatenate([key_high, key_low, query_high, query_low], axis=0))
+            fetch(step).wait()
+            memory = held[spot].reshape(count * size, size).astype(jnp.bfloat16)
+            both = jnp.dot(wide, memory, preferred_element_type=jnp.float32)
+            recalled = both[0:count] + both[count : 2 * count]
+            asked = both[2 * count : 3 * count] + both[3 * count : 4 * count]
+            factors = packed[spot, 2 * size : 3 * size]
+            change = work[near, 3 * size : 4 * size] * (
+                work[near, size : 2 * size] - factors * recalled
+            )
+            packed[spot, size : 2 * size] = change
+            read = factors * asked + work[near, 4 * size : 5 * size] * change
+            scaling = lax.rsqrt(jnp.sum(read * read, axis=1, keepdims=True) / size + EPS)
+            gated[c, near, :] = (read * scaling * work[near, 2 * size : 3 * size]).astype(
+                jnp.bfloat16
+            )
+            return carry
+
+        lax.fori_loop(0, chip_rows // count, body, 0)
+        span = pl.ds(c * rows, rows)
+        same = gated.at[c, pl.ds(pl.multiple_of(core * rows, rows), rows), :]
+        cross = gated.at[c, pl.ds(pl.multiple_of((1 - core) * rows, rows), rows), :]
+        for i, (source, phase, j, device) in enumerate(
+            (
+                (same, 1, 0, partner),
+                (cross, 1, 1, partner_sibling),
+                (cross, 0, 1, sibling),
+            )
+        ):
+            copy = remote(
+                source,
+                left.at[phase, span, j * size : (j + 1) * size],
+                gated_send.at[c, i],
+                gated_recv.at[c, i],
+                device,
+            )
+            copy.start()
+            shares.append(copy)
+        left[0, c * rows : (c + 1) * rows, 0:size] = gated[
+            c, pl.ds(pl.multiple_of(core * rows, rows), rows), :
+        ]
+
+    wide_half = cols // 2
+    turns = [(1, 2), (2, 1)]
+    hops = []
+
+    def expand(phase):
+        lefts = left[phase]
+        for p, (first, second) in enumerate(turns):
+            span = slice(p * wide_half, (p + 1) * wide_half)
+            product = lax.dot_general(
+                lefts,
+                both_w[span, :],
+                (((1,), (1,)), ((), ())),
+                preferred_element_type=jnp.float32,
+            )
+            for i, c in enumerate((first + second, first)):
+                hop_out[phase, p, i] = product[c * rows : (c + 1) * rows].astype(jnp.bfloat16)
+                copy = hop(phase, p, i)
+                copy.start()
+                hops.append(copy)
+            acc[phase, 0, :, span] = product[0:rows]
+            acc[phase, 1, :, span] = product[second * rows : (second + 1) * rows]
+
+    def hop(phase, p, i):
+        return remote(
+            hop_out.at[phase, p, i],
+            hop_in.at[phase, p, i],
+            hop_send.at[phase, p, i],
+            hop_recv.at[phase, p, i],
+            neighbours[turns[p][0] - 1],
+        )
+
+    def last(phase, p):
+        return remote(
+            last_out.at[phase, p],
+            last_in.at[phase, p],
+            last_send.at[phase, p],
+            last_recv.at[phase, p],
+            neighbours[turns[p][1] - 1],
+        )
+
+    def up(p):
+        return remote(
+            up_out.at[p], up_in.at[p], up_send.at[p], up_recv.at[p], neighbours[top - 1]
+        )
+
+    def second_hop(phase):
+        for p in range(2):
+            span = slice(p * wide_half, (p + 1) * wide_half)
+            hop(phase, p, 0).wait_recv()
+            last_out[phase, p] = (
+                acc[phase, 1, :, span] + hop_in[phase, p, 0].astype(jnp.float32)
+            ).astype(jnp.bfloat16)
+            last(phase, p).start()
+        for p in range(2):
+            span = slice(p * wide_half, (p + 1) * wide_half)
+            hop(phase, p, 1).wait_recv()
+            acc[phase, 0, :, span] += hop_in[phase, p, 1].astype(jnp.float32)
+
+    def settle(phase):
+        for p in range(2):
+            span = slice(p * wide_half, (p + 1) * wide_half)
+            last(phase, p).wait_recv()
+            total = acc[phase, 0, :, span] + last_in[phase, p].astype(jnp.float32)
+
+            @pl.when(keep == phase)
+            def _():
+                acc[phase, 0, :, span] = total
+
+            @pl.when(keep != phase)
+            def _():
+                up_out[p] = total.astype(jnp.bfloat16)
+                up(p).start()
+
+    x, y, z = 1, 2, flats
+    project(0)
+    other_half.start()
+    relay(0, z)
+    relay(0, x)
+    relay(1, z)
+    relay(1, y)
+    relay(0, y)
+    relay(1, x)
+    project(z)
+    relay(0, x + z)
+    project(x)
+    relay(1, y + z)
+    relay(1, x + z)
+    relay(0, y + z)
+    project(y)
+    relay(0, x + y)
+    relay(1, x + y)
+    project(x + z)
+    project(y + z)
+    project(x + y)
+    recall(0)
+    relay(0, x + y + z)
+    relay(1, x + y + z)
+    project(x + y + z)
+    for c in range(1, flats):
+        recall(c)
+    own_half.wait()
+    other_half.wait_recv()
+    for c in range(flats):
+        shares[3 * c + 2].wait_recv()
+    expand(0)
+    for c in range(flats):
+        shares[3 * c].wait_recv()
+        shares[3 * c + 1].wait_recv()
+    expand(1)
+    second_hop(0)
+    second_hop(1)
+    settle(0)
+    settle(1)
+    for p in range(2):
+        span = slice(p * wide_half, (p + 1) * wide_half)
+        up(p).wait_recv()
+        result[:, span] = (
+            stream_ref[:, span].astype(jnp.float32)
+            + acc[keep, 0, :, span]
+            + up_in[p].astype(jnp.float32)
+        ).astype(jnp.bfloat16)
+    for copy in sends + main_copies + small_copies + shares + hops + [other_half]:
+        copy.wait_send()
+    for p in range(2):
+        up(p).wait_send()
+        for phase in range(2):
+            last(phase, p).wait_send()
+
+
+def fused(stream, norm_gain, weights, write_weight, decay_weight, rate, head_gain, out_weight, state, groups):
+    rows, cols = stream.shape
+    heads = rate.shape[0]
+    size = weights[0].shape[1]
+    dims = heads.bit_length() - 2
+    flats = (1 << dims) // 2
+    group_rows = state.shape[0]
+    steps = group_rows // min(16, group_rows)
+    batch = rows * heads
+    chip_rows = 2 * rows
+    dma = pltpu.SemaphoreType.DMA
+    anywhere = pl.BlockSpec(memory_space=pltpu.HBM)
+    f32, bf16 = jnp.float32, jnp.bfloat16
+    return pl.pallas_call(
+        functools.partial(fused_kernel, heads, groups),
+        in_specs=[VMEM] * 2 + [anywhere] * 6 + [VMEM] * 2 + [anywhere] * 2,
+        out_specs=[VMEM] * 3,
+        out_shape=[
+            pltpu.VMEM(state.shape, state.dtype),
+            pltpu.VMEM((group_rows, 3 * size), f32),
+            pltpu.VMEM(stream.shape, stream.dtype),
+        ],
+        scratch_shapes=[
+            pltpu.VMEM((batch, cols), bf16),
+            pltpu.VMEM((cols, 4 * size), bf16),
+            pltpu.VMEM((2 * heads, cols), bf16),
+            pltpu.VMEM((1, cols), f32),
+            pltpu.VMEM((groups * cols // 128, 128), f32),
+            pltpu.VMEM((cols, 2 * size), bf16),
+            pltpu.VMEM((flats, chip_rows, 4 * size), f32),
+            pltpu.VMEM((flats, chip_rows, 128), f32),
+            pltpu.VMEM((flats, chip_rows, 4 * size), bf16),
+            pltpu.VMEM((flats, chip_rows, 4 * size), bf16),
+            pltpu.VMEM((flats, SMALL, max(128, chip_rows)), bf16),
+            pltpu.VMEM((flats, SMALL, max(128, chip_rows)), bf16),
+            pltpu.VMEM((chip_rows, 5 * size), f32),
+            pltpu.VMEM((flats, chip_rows, size), bf16),
+            pltpu.VMEM((2, flats * rows, 2 * size), bf16),
+            pltpu.VMEM((2, 2, rows, cols), f32),
+            pltpu.VMEM((2, 2, 2, rows, cols // 2), bf16),
+            pltpu.VMEM((2, 2, 2, rows, cols // 2), bf16),
+            pltpu.VMEM((2, 2, rows, cols // 2), bf16),
+            pltpu.VMEM((2, 2, rows, cols // 2), bf16),
+            pltpu.VMEM((2, rows, cols // 2), bf16),
+            pltpu.VMEM((2, rows, cols // 2), bf16),
+            dma((7,)),
+            dma((steps,)),
+            dma((2,)),
+            dma((2, 2 * flats)),
+            dma((2, 2 * flats)),
+            dma((2, 2 * flats)),
+            dma((2, 2 * flats)),
+            dma((flats,)),
+            dma((flats,)),
+            dma((flats,)),
+            dma((flats,)),
+            dma((flats, 3)),
+            dma((flats, 3)),
+            dma((2, 2, 2)),
+            dma((2, 2, 2)),
+            dma((2, 2)),
+            dma((2, 2)),
+            dma((2,)),
+            dma((2,)),
+        ],
+        compiler_params=pltpu.CompilerParams(
+            collective_id=2, has_side_effects=True, vmem_limit_bytes=43 << 20
+        ),
+    )(
+        stream,
+        norm_gain.reshape(groups * cols // 128, 128),
+        *weights,
+        write_weight.T,
+        decay_weight.T,
+        rate.reshape(1, heads),
+        head_gain.reshape(1, size),
+        out_weight,
+        state,
+    )
+
+
+def store_kernel(held, packed, result, new_ref, out_ref, fresh, sems, out_sem):
+    total, size, _ = held.shape
+    steps = sems.shape[0]
+    count = total // steps
+    copy_out = pltpu.make_async_copy(result, out_ref, out_sem)
+    copy_out.start()
+
+    def store(step):
+        spot = pl.ds(pl.multiple_of(step * count, count), count)
+        return pltpu.make_async_copy(fresh.at[spot], new_ref.at[spot], sems.at[step])
+
+    spots = lax.broadcasted_iota(jnp.int32, (3 * count, size), 0) % count
+
+    def body(step, carry):
+        spot = pl.ds(pl.multiple_of(step * count, count), count)
+        key_high, key_low = split(packed[spot, 0:size])
+        change_high, change_low = split(packed[spot, size : 2 * size])
+        factor = packed[spot, 2 * size : 3 * size]
+        keys = jnp.concatenate([key_high, key_low, key_high], axis=0)
+        keys = jnp.concatenate([keys, jnp.zeros((size - 3 * count, size), keys.dtype)], axis=0)
+        keys = keys.astype(jnp.float32).T.astype(jnp.bfloat16)[:, 0 : 3 * count]
+        changes = jnp.concatenate([change_high, change_high, change_low], axis=0)
+        wide = jnp.concatenate(
+            [jnp.where(spots == b, changes, jnp.zeros_like(changes)) for b in range(count)], axis=1
+        )
+        outer = jnp.dot(keys, wide, preferred_element_type=jnp.float32)
+        for b in range(count):
+            fresh[step * count + b] = (
+                factor[b : b + 1, :] * held[step * count + b]
+                + outer[:, b * size : (b + 1) * size]
+            )
+        store(step).start()
+        return carry
+
+    lax.fori_loop(0, steps, body, 0)
+    for step in range(steps):
+        store(step).wait()
+    copy_out.wait()
+
+
+def store(held, packed, result):
+    total = held.shape[0]
+    steps = total // min(16, total)
+    anywhere = pl.BlockSpec(memory_space=pl.ANY)
+    return pl.pallas_call(
+        store_kernel,
+        in_specs=[VMEM] * 3,
+        out_specs=[anywhere] * 2,
+        out_shape=[
+            jax.ShapeDtypeStruct(held.shape, held.dtype),
+            jax.ShapeDtypeStruct(result.shape, result.dtype),
+        ],
+        scratch_shapes=[
+            pltpu.VMEM(held.shape, held.dtype),
+            pltpu.SemaphoreType.DMA((steps,)),
+            pltpu.SemaphoreType.DMA(()),
+        ],
+        compiler_params=pltpu.CompilerParams(vmem_limit_bytes=20 << 20),
+    )(held, packed, result)
+
+
 def per_device(
     stream,
     norm_gain,
@@ -657,6 +1232,22 @@
     heads = decay_rate.shape[0]
     groups = lax.axis_size("tp") // heads
     weights = (query_weight, key_weight, value_weight, gate_weight)
+    rows, cols = stream.shape
+    if groups == 2 and heads == 16 and rows % 32 == 0 and rows <= 64 and cols % 256 == 0:
+        held, packed, result = fused(
+            stream,
+            norm_gain,
+            weights,
+            write_weight,
+            decay_weight,
+            decay_rate,
+            head_gain,
+            out_weight,
+            state,
+            groups,
+        )
+        updated, result = store(held, packed, result)
+        return (result, updated)
     packed = project(
         stream, norm_gain, weights, write_weight, decay_weight, decay_rate, heads, groups
     )

time: 72.2 us -> 52.7 us (0.73)
  Pallas kernels: 69.8 us -> 51.9 us
  local copies, waits for them, and re-layouts: 1.57 us -> 0 us
    pallas_call x3 -> x2, Pallas kernels: 69.8 us -> 51.9 us  [the longest x1 45.2 us: fused(): pl.pallas_call(functools.partial(fused_kernel, heads, groups), in_specs=[...]
    unnamed x1 -> x0, local copies, waits for them, and re-layouts: 1.57 us -> none
where the time goes in v1:
time: 52.7 us; the launch traced here: 52.5 us
  Pallas kernels  51.9 us (98%)
  between operations  0.64 us (1%)
    pallas_call x1, Pallas kernels, fused(): pl.pallas_call(functools.partial(fused_kernel, heads, groups), in_specs=[...  45.2 us
    pallas_call x1, Pallas kernels, store(): pl.pallas_call(store_kernel, in_specs=[VMEM] * 3, out_specs=[anywhere] *...  6.65 us

profile of v1, /device:TPU:0, one launch (start us, length us, event | category | flops | bytes accessed | tf_op | source)
XLA Modules:
  0.0 52.5 jit_solution(15062276705878172625)
XLA Ops:
  0.6 45.2 %shard_map.131 = (f32[256,128,128]{2,1,0:T(8,128)S(1)}, f32[256,384]{1,0:T(8,128)S(1)}, bf16[32,2048]{1,0:T(8,128)(2,1)S(1)}) custom-call(bf16[32,2048]{1,0:T(8,128)(2,1)} %stream_ref.1, bf16[32,128]{1,0:T(8,128)(2,1)} %bitcast.7, bf16[2048,128]{1,0:T(8,128)(2,1)} %query_w.1, bf16[2048,128]{1,0:T(8,128)(2,1)} %key_w.1, bf16[2048,128]{1,0:T(8,128)(2,1)} %value_w.1, ...), custom_call_target="tpu_custom_call" | custom-call | tf_op jit(solution)/shard_map/pallas_call | solution.py:1089
  45.8 6.7 %shard_map.132 = (f32[256,128,128]{2,1,0:T(8,128)}, bf16[32,2048]{1,0:T(8,128)(2,1)}) custom-call(f32[256,128,128]{2,1,0:T(8,128)S(1)} %get-tuple-element.7.held, f32[256,384]{1,0:T(8,128)S(1)} %get-tuple-element.8.packed, bf16[32,2048]{1,0:T(8,128)(2,1)S(1)} %get-tuple-element.9.result), custom_call_target="tpu_custom_call" | custom-call | tf_op jit(solution)/shard_map/pallas_call | solution.py:1201

commit v2 on v0

--- a/solution.py
+++ b/solution.py
@@ -640,6 +640,608 @@
     )(stream, gated, scaling, out_weight)
 
 
+def masked(mask, dims):
+    return tuple(bit for bit in range(1, dims + 1) if mask >> (bit - 1) & 1)
+
+
+def fused_kernel(
+    heads,
+    groups,
+    stream_hbm,
+    gain_hbm,
+    query_w,
+    key_w,
+    value_w,
+    gate_w,
+    write_w,
+    decay_w,
+    rate_hbm,
+    head_gain_hbm,
+    out_w,
+    state_ref,
+    held,
+    mine_out,
+    rise_out,
+    stream_ref,
+    gain_ref,
+    rate_ref,
+    head_gain_ref,
+    gathered,
+    weights,
+    side_w,
+    gain_row,
+    gains,
+    four_w,
+    partial,
+    partial_side,
+    sent,
+    received,
+    small_sent,
+    small_received,
+    packed,
+    answers,
+    gated,
+    left,
+    acc,
+    hop_out,
+    hop_in,
+    local_sems,
+    state_sems,
+    pair_sems,
+    send_sems,
+    ici_recv,
+    core_recv,
+    main_recv,
+    small_recv,
+    gated_recv,
+    hop_recv,
+):
+    me = lax.axis_index("tp")
+    place = me % heads
+    group = me // heads
+    core = place % 2
+    rows, cols = stream_ref.shape
+    size = query_w.shape[1]
+    dims = heads.bit_length() - 2
+    chips = 1 << dims
+    flats = chips // 2
+    chip_rows = 2 * rows
+    group_rows = flats * chip_rows
+    count = 16
+    x, y, z = 1, 2, flats
+    sibling = flip(me, (0,))
+    neighbours = [flip(me, (bit,)) for bit in range(1, dims + 1)]
+    partner = place + heads * ((group + 1) % groups)
+    peers = [sibling] + neighbours + [partner, flip(partner, (0,))]
+    for h in range(2):
+        there = flip(partner, (h + 1,))
+        peers += [flip(neighbours[h], (0,)), there, flip(there, (0,))]
+    own_cols = pl.ds(pl.multiple_of(group * cols, cols), cols)
+    upper = place // flats // 2
+    keep = (upper + group) % 2
+    outer = 1 - keep
+
+    barrier = pltpu.get_barrier_semaphore()
+    for device in peers:
+        pl.semaphore_signal(barrier, inc=1, device_id=(device,), device_id_type=MESH)
+    early = [
+        pltpu.make_async_copy(source, target, local_sems.at[i])
+        for i, (source, target) in enumerate(
+            (
+                (stream_hbm, stream_ref),
+                (gain_hbm, gain_ref),
+                (rate_hbm, rate_ref),
+                (head_gain_hbm, head_gain_ref),
+            )
+        )
+    ]
+    for copy in early:
+        copy.start()
+    for i, weight in enumerate((query_w, key_w, value_w, gate_w)):
+        pltpu.make_async_copy(
+            weight, weights.at[:, i * size : (i + 1) * size], local_sems.at[4]
+        ).start()
+    for i, source in enumerate((write_w, decay_w)):
+        pltpu.make_async_copy(
+            source.at[:, own_cols], side_w.at[i * heads : (i + 1) * heads], local_sems.at[5]
+        ).start()
+    weights_done = pltpu.make_async_copy(weights, weights, local_sems.at[4])
+    side_done = pltpu.make_async_copy(side_w, side_w, local_sems.at[5])
+    own_w = pltpu.make_async_copy(out_w, four_w.at[:, 0:size], local_sems.at[6])
+    sibling_w = remote(
+        out_w, four_w.at[:, size : 2 * size], pair_sems.at[0], pair_sems.at[1], sibling
+    )
+    pieces = 4
+    wide_half = cols // 2
+    tall = wide_half // pieces
+
+    def beside_w(h, i, n=1):
+        spot = slice(h * wide_half + i * tall, h * wide_half + (i + n) * tall)
+        return remote(
+            out_w.at[spot, :],
+            four_w.at[spot, 2 * size : 3 * size],
+            pair_sems.at[3],
+            pair_sems.at[4 + h],
+            neighbours[h],
+        )
+
+    def passed_w(h, n=1):
+        spot = slice(h * wide_half, (h + n) * wide_half)
+        return remote(
+            four_w.at[spot, 2 * size : 3 * size],
+            four_w.at[spot, 3 * size : 4 * size],
+            pair_sems.at[2],
+            pair_sems.at[6],
+            sibling,
+        )
+
+    def fetch(c):
+        spot = pl.ds(pl.multiple_of(c * chip_rows, chip_rows), chip_rows)
+        return pltpu.make_async_copy(state_ref.at[spot], held.at[spot], state_sems.at[c])
+
+    half = rows // 2
+    top = dims
+    parts = [(0, (top, 1, 2)), (half, (top, 2, 1))]
+
+    def block(device_place, p, q):
+        begin = device_place * rows + parts[p][0]
+        return gathered.at[
+            pl.ds(pl.multiple_of(begin, half), half), q * wide_half : (q + 1) * wide_half
+        ]
+
+    def pass_on(p, q, bits):
+        order = parts[p][1]
+        step = max([order.index(bit) for bit in bits], default=-1)
+        target = block(flip(place, bits), p, q)
+        source = target
+        if not bits:
+            source = stream_ref.at[
+                parts[p][0] : parts[p][0] + half, q * wide_half : (q + 1) * wide_half
+            ]
+        for later in range(step + 1, dims):
+            remote(
+                source,
+                target,
+                send_sems.at[0],
+                ici_recv.at[p, q, key_of(bits + (order[later],)) - 1],
+                flip(me, (order[later],)),
+            ).start()
+        remote(source, target, send_sems.at[1], core_recv.at[key_of(bits)], sibling).start()
+
+    def relay(p, q, mask):
+        bits = masked(mask, dims)
+        target = block(flip(place, bits), p, q)
+        remote(target, target, send_sems.at[0], ici_recv.at[p, q, mask - 1], sibling).wait_recv()
+        pass_on(p, q, bits)
+
+    spot_x, spot_y = place // 2 % 2, place // 4 % 2
+
+    def chip_of(c):
+        return (spot_x + c) % 2 + 2 * ((spot_y + c // 2) % 2)
+
+    def from_sibling(c, raised):
+        level = (upper + raised) % 2
+        begin = (level * flats + chip_of(c)) * chip_rows + (1 - core) * rows
+        target = gathered.at[pl.ds(pl.multiple_of(begin, rows), rows), :]
+        remote(
+            target, target, send_sems.at[1], core_recv.at[c + flats * raised], sibling
+        ).wait_recv()
+
+    for copy in early:
+        copy.wait()
+    pl.semaphore_wait(barrier, len(peers))
+    for q in range(2):
+        for p in range(2):
+            pass_on(p, q, ())
+    sibling_w.start()
+    gathered[pl.ds(pl.multiple_of(place * rows, rows), rows), :] = stream_ref[...]
+    gains[...] = gain_ref[...].astype(jnp.float32)
+    tiles = cols // 128
+    for i in range(tiles):
+        gain_row[:, i * 128 : (i + 1) * 128] = gains[pl.ds(group * tiles + i, 1), :]
+    weights_done.wait()
+    side_done.wait()
+    for c in range(flats):
+        fetch(chip_of(c)).start()
+    own_w.start()
+
+    def project(begin, high):
+        x = gathered[pl.ds(pl.multiple_of(begin, chip_rows), high), :].astype(jnp.float32)
+        gained = (x * gain_row[...]).astype(jnp.bfloat16)
+        product = jnp.dot(gained, weights[...], preferred_element_type=jnp.float32)
+        pre = lax.dot_general(
+            gained, side_w[...], (((1,), (1,)), ((), ())), preferred_element_type=jnp.float32
+        )
+        spot = lax.broadcasted_iota(jnp.int32, pre.shape, 1)
+        write = jnp.sum(jnp.where(spot == place, pre, 0.0), axis=1, keepdims=True)
+        decay = jnp.sum(jnp.where(spot == place + heads, pre, 0.0), axis=1, keepdims=True)
+        squares = jnp.sum(x * x, axis=1, keepdims=True)
+        lane = lax.broadcasted_iota(jnp.int32, (high, 128), 1)
+        side = jnp.where(
+            lane == 0, write, jnp.where(lane == 1, decay, jnp.where(lane == 2, squares, 0.0))
+        )
+        return product, side
+
+    away_begin = (group + 1) % groups * group_rows
+
+    def main_copy(c):
+        return remote(sent.at[c], received.at[c], send_sems.at[2], main_recv.at[c], partner)
+
+    def small_copy(c):
+        return remote(
+            small_sent.at[c], small_received.at[c], send_sems.at[3], small_recv.at[c], partner
+        )
+
+    def project_away(c, raised):
+        from_sibling(c, raised)
+        product, side = project(away_begin + chip_of(c) * chip_rows, chip_rows)
+        sent[c] = product.astype(jnp.bfloat16)
+        main_copy(c).start()
+        if chip_rows < 128:
+            side = jnp.concatenate(
+                [side, jnp.zeros((128 - chip_rows, 128), jnp.float32)], axis=0
+            )
+        small_sent[c] = side.T[0:SMALL].astype(jnp.bfloat16)
+        small_copy(c).start()
+
+    def project_here(j, raised):
+        for c in range(2 * j, 2 * j + 2):
+            from_sibling(c, raised)
+        pair = (spot_y + j) % 2
+        spot = pl.ds(pl.multiple_of(pair * 2 * chip_rows, 2 * chip_rows), 2 * chip_rows)
+        product, side = project(group * group_rows + pair * 2 * chip_rows, 2 * chip_rows)
+        partial[spot, :] = product
+        partial_side[spot, :] = side
+
+    def marks(n):
+        return lax.broadcasted_iota(jnp.int32, (n * count, size), 0) % count
+
+    def diagonal(values, spots):
+        return jnp.concatenate(
+            [jnp.where(spots == b, values, jnp.zeros_like(values)) for b in range(count)], axis=1
+        )
+
+    def rounded(v):
+        return v.astype(jnp.bfloat16).astype(jnp.float32)
+
+    mine = lax.broadcasted_iota(jnp.int32, rate_ref.shape, 1) == place
+    rate = jnp.sum(jnp.where(mine, rate_ref[...], 0.0), axis=1, keepdims=True)
+
+    def recall(c):
+        main_copy(c).wait_recv()
+        small_copy(c).wait_recv()
+        begin = chip_of(c) * chip_rows
+        whole = pl.ds(pl.multiple_of(begin, chip_rows), chip_rows)
+        total = partial[whole, :] + received[c].astype(jnp.float32)
+        flat = small_received[c].astype(jnp.float32)
+        flat = jnp.concatenate([flat, jnp.zeros((128 - SMALL, flat.shape[1]), jnp.float32)], axis=0)
+        side = partial_side[whole, :] + flat.T[0:chip_rows]
+        scale = lax.rsqrt(side[:, 2:3] / (cols * groups) + EPS)
+        projected = rounded(total * scale)
+        query = projected[:, :size]
+        key = projected[:, size : 2 * size]
+        query = query * lax.rsqrt(jnp.sum(query * query, axis=1, keepdims=True) + EPS) * size**-0.5
+        key = key * lax.rsqrt(jnp.sum(key * key, axis=1, keepdims=True) + EPS)
+        key_high, key_low = split(key)
+        query_high, query_low = split(query)
+        fetch(chip_of(c)).wait()
+        spots = marks(4)
+        for i in range(chip_rows // count):
+            near = slice(i * count, (i + 1) * count)
+            spot = pl.ds(pl.multiple_of(begin + i * count, count), count)
+            four = [v[near] for v in (key_high, key_low, query_high, query_low)]
+            wide = diagonal(jnp.concatenate(four, axis=0), spots)
+            memory = held[spot].reshape(count * size, size).astype(jnp.bfloat16)
+            both = jnp.dot(wide, memory, preferred_element_type=jnp.float32)
+            answers[0, near, :] = both[0:count] + both[count : 2 * count]
+            answers[1, near, :] = both[2 * count : 3 * count] + both[3 * count : 4 * count]
+        pre = rounded(side * scale)
+        strength = jax.nn.sigmoid(pre[:, 0:1])
+        decay = pre[:, 1:2]
+        softplus = jnp.maximum(decay, 0.0) + jnp.log(1.0 + jnp.exp(-jnp.abs(decay)))
+        factor = jnp.broadcast_to(jnp.exp(-rate * softplus), (chip_rows, size))
+        overlap = jnp.sum(query * key, axis=1, keepdims=True)
+        gate = projected[:, 3 * size :]
+        lift = head_gain_ref[...].astype(jnp.float32) * (gate / (1.0 + jnp.exp(-gate)))
+        change = strength * (projected[:, 2 * size : 3 * size] - factor * answers[0])
+        read = factor * answers[1] + overlap * change
+        scaling = lax.rsqrt(jnp.sum(read * read, axis=1, keepdims=True) / size + EPS)
+        gated[c] = (read * scaling * lift).astype(jnp.bfloat16)
+        same = gated.at[c, pl.ds(pl.multiple_of(core * rows, rows), rows), :]
+        cross = gated.at[c, pl.ds(pl.multiple_of((1 - core) * rows, rows), rows), :]
+        for h in range(2 if c else 1):
+            gap, row = (c // 2, c % 2) if h else (c % 2, c // 2)
+            span = slice(row * rows, (row + 1) * rows)
+            first = 2 * gap
+            there = flip(partner, (h + 1,)) if gap else partner
+            here = neighbours[h] if gap else me
+            for source, phase, j, device in (
+                (same, 1, first, there),
+                (cross, 1, first + 1, flip(there, (0,))),
+                (cross, 0, first + 1, flip(here, (0,))),
+                (same, 0, first, here),
+            ):
+                target = left.at[h, phase, span, j * size : (j + 1) * size]
+                if phase or j:
+                    remote(source, target, send_sems.at[4], gated_recv.at[h, phase], device).start()
+                else:
+                    left[h, 0, span, 0:size] = gated[
+                        c, pl.ds(pl.multiple_of(core * rows, rows), rows), :
+                    ]
+        packed[c, 0] = key
+        packed[c, 1] = change
+        packed[c, 2] = factor
+
+    def update(c):
+        begin = chip_of(c) * chip_rows
+        spots = marks(3)
+
+        def body(i, carry):
+            near = pl.ds(pl.multiple_of(i * count, count), count)
+            key_high, key_low = split(packed[c, 0, near, :])
+            change_high, change_low = split(packed[c, 1, near, :])
+            factor = packed[c, 2, near, :]
+            keys = jnp.concatenate([key_high, key_low, key_high], axis=0)
+            keys = jnp.concatenate([keys, jnp.zeros((size - 3 * count, size), keys.dtype)], axis=0)
+            keys = keys.astype(jnp.float32).T.astype(jnp.bfloat16)[:, 0 : 3 * count]
+            wide = diagonal(jnp.concatenate([change_high, change_high, change_low], axis=0), spots)
+            outer_product = jnp.dot(keys, wide, preferred_element_type=jnp.float32)
+            for b in range(count):
+                spot = begin + i * count + b
+                held[spot] = (
+                    factor[b : b + 1, :] * held[spot]
+                    + outer_product[:, b * size : (b + 1) * size]
+                )
+            return carry
+
+        lax.fori_loop(0, chip_rows // count, body, 0)
+
+    def hop(phase, h):
+        return remote(
+            hop_out.at[phase, h],
+            hop_in.at[phase, h],
+            send_sems.at[5],
+            hop_recv.at[phase, h],
+            neighbours[1 - h],
+        )
+
+    def expand(phase):
+        for h in range(2):
+            span = slice(h * wide_half, (h + 1) * wide_half)
+            lefts = left[h, phase]
+            if h:
+                upper_rows = jnp.concatenate(
+                    [left[0, phase, 0:rows, 0 : 2 * size], lefts[0:rows, 2 * size :]], axis=1
+                )
+                lefts = jnp.concatenate([upper_rows, lefts[rows:]], axis=0)
+            product = lax.dot_general(
+                lefts,
+                four_w[span, :],
+                (((1,), (1,)), ((), ())),
+                preferred_element_type=jnp.float32,
+            )
+            hop_out[phase, h] = product[rows:].astype(jnp.bfloat16)
+            hop(phase, h).start()
+            acc[phase, :, span] = product[0:rows]
+
+    def settle(phase):
+        for q in range(2):
+            span = slice(q * wide_half, (q + 1) * wide_half)
+            hop(phase, q).wait_recv()
+            total = acc[phase, :, span] + hop_in[phase, q].astype(jnp.float32)
+
+            @pl.when(keep == phase)
+            def _():
+                mine_out[:, span] = total
+
+            @pl.when(keep != phase)
+            def _():
+                rise_out[:, span] = total.astype(jnp.bfloat16)
+
+    def gated_bytes(h, phase):
+        blocks = (6, 8) if h == 0 else (5, 6)
+        return gathered.at[0:rows, 0 : blocks[phase] * size]
+
+    def whole_left(phase):
+        for h in range(2):
+            target = gated_bytes(h, phase)
+            remote(target, target, send_sems.at[4], gated_recv.at[h, phase], sibling).wait_recv()
+
+    def relays(masks):
+        for q in range(2):
+            for p, mask in masks:
+                relay(p, q, mask)
+
+    def send_beside(first, last):
+        for i in range(first, last):
+            for h in range(2):
+                beside_w(h, i).start()
+
+    def pass_weights(h):
+        beside_w(h, 0, pieces).wait_recv()
+        passed_w(h).start()
+
+    def weights_ready():
+        own_w.wait()
+        sibling_w.wait_recv()
+        passed_w(0, 2).wait_recv()
+
+    def drain():
+        sibling_w.wait_send()
+        passed_w(0, 2).wait_send()
+        for h in range(2):
+            beside_w(h, 0, pieces).wait_send()
+        ici_rows = rows * (chips - 1)
+        for i, ref in enumerate(
+            (gathered.at[0:ici_rows, :], gathered.at[0 : rows * chips, :], sent, small_sent)
+        ):
+            remote(ref, ref, send_sems.at[i], main_recv.at[0], partner).wait_send()
+        for phase in range(2):
+            for h in range(2):
+                target = gated_bytes(h, phase)
+                remote(target, target, send_sems.at[4], gated_recv.at[0, 0], sibling).wait_send()
+        remote(hop_out, hop_in, send_sems.at[5], hop_recv.at[0, 0], sibling).wait_send()
+
+    @pl.when(outer == 1)
+    def _():
+        relays([(0, z), (1, z)])
+        project_away(0, 1)
+        relays([(0, x), (1, y), (1, x), (0, y)])
+        send_beside(0, 1)
+        relays([(0, x + z), (1, y + z), (1, x + z), (0, y + z)])
+        project_away(1, 1)
+        project_away(2, 1)
+        send_beside(1, pieces)
+        project_here(0, 0)
+        relays([(0, x + y + z), (1, x + y + z)])
+        project_away(3, 1)
+        relays([(0, x + y), (1, x + y)])
+        project_here(1, 0)
+
+    @pl.when(outer == 0)
+    def _():
+        project_away(0, 0)
+        relays([(0, x), (1, y), (1, x), (0, y)])
+        project_away(1, 0)
+        project_away(2, 0)
+        relays([(0, z), (1, z)])
+        relays([(0, x + y), (1, x + y)])
+        project_away(3, 0)
+        relays([(0, x + z), (1, y + z), (1, x + z), (0, y + z)])
+        send_beside(0, pieces)
+        project_here(0, 1)
+        relays([(0, x + y + z), (1, x + y + z)])
+        project_here(1, 1)
+
+    recall(0)
+    recall(1)
+    recall(2)
+    recall(3)
+    pass_weights(0)
+    pass_weights(1)
+    weights_ready()
+    whole_left(0)
+    expand(0)
+    update(0)
+    update(1)
+    whole_left(1)
+    expand(1)
+    update(2)
+    settle(0)
+    update(3)
+    settle(1)
+    drain()
+
+
+def fused(
+    stream,
+    norm_gain,
+    weights,
+    write_weight,
+    decay_weight,
+    rate,
+    head_gain,
+    out_weight,
+    state,
+    groups,
+):
+    rows, cols = stream.shape
+    heads = rate.shape[0]
+    size = weights[0].shape[1]
+    chips = heads // 2
+    flats = chips // 2
+    batch = rows * heads
+    chip_rows = 2 * rows
+    dma = pltpu.SemaphoreType.DMA
+    anywhere = pl.BlockSpec(memory_space=pltpu.HBM)
+    f32, bf16 = jnp.float32, jnp.bfloat16
+    return pl.pallas_call(
+        functools.partial(fused_kernel, heads, groups),
+        in_specs=[anywhere] * 12,
+        out_specs=[VMEM] * 3,
+        out_shape=[
+            pltpu.VMEM(state.shape, state.dtype),
+            pltpu.VMEM(stream.shape, f32),
+            pltpu.VMEM(stream.shape, bf16),
+        ],
+        scratch_shapes=[
+            pltpu.VMEM(stream.shape, stream.dtype),
+            pltpu.VMEM((groups * cols // 128, 128), bf16),
+            pltpu.VMEM((1, heads), f32),
+            pltpu.VMEM((1, size), bf16),
+            pltpu.VMEM((batch, cols), bf16),
+            pltpu.VMEM((cols, 4 * size), bf16),
+            pltpu.VMEM((2 * heads, cols), bf16),
+            pltpu.VMEM((1, cols), f32),
+            pltpu.VMEM((groups * cols // 128, 128), f32),
+            pltpu.VMEM((cols, 4 * size), bf16),
+            pltpu.VMEM((flats * chip_rows, 4 * size), f32),
+            pltpu.VMEM((flats * chip_rows, 128), f32),
+            pltpu.VMEM((flats, chip_rows, 4 * size), bf16),
+            pltpu.VMEM((flats, chip_rows, 4 * size), bf16),
+            pltpu.VMEM((flats, SMALL, max(128, chip_rows)), bf16),
+            pltpu.VMEM((flats, SMALL, max(128, chip_rows)), bf16),
+            pltpu.VMEM((flats, 3, chip_rows, size), f32),
+            pltpu.VMEM((2, chip_rows, size), f32),
+            pltpu.VMEM((flats, chip_rows, size), bf16),
+            pltpu.VMEM((2, 2, 2 * rows, 4 * size), bf16),
+            pltpu.VMEM((2, rows, cols), f32),
+            pltpu.VMEM((2, 2, rows, cols // 2), bf16),
+            pltpu.VMEM((2, 2, rows, cols // 2), bf16),
+            dma((7,)),
+            dma((flats,)),
+            dma((7,)),
+            dma((6,)),
+            dma((2, 2, chips - 1)),
+            dma((chips,)),
+            dma((flats,)),
+            dma((flats,)),
+            dma((2, 2)),
+            dma((2, 2)),
+        ],
+        compiler_params=pltpu.CompilerParams(
+            collective_id=2, has_side_effects=True, vmem_limit_bytes=43 << 20
+        ),
+    )(
+        stream,
+        norm_gain.reshape(groups * cols // 128, 128),
+        *weights,
+        write_weight.T,
+        decay_weight.T,
+        rate.reshape(1, heads),
+        head_gain.reshape(1, size),
+        out_weight,
+        state,
+    )
+
+
+def store_kernel(held, new_ref, sems):
+    steps = sems.shape[0]
+    count = held.shape[0] // steps
+    copies = []
+    for step in range(steps):
+        spot = slice(step * count, (step + 1) * count)
+        copies.append(pltpu.make_async_copy(held.at[spot], new_ref.at[spot], sems.at[step]))
+        copies[-1].start()
+    for copy in copies:
+        copy.wait()
+
+
+def store(held):
+    steps = min(8, held.shape[0])
+    return pl.pallas_call(
+        store_kernel,
+        in_specs=[VMEM],
+        out_specs=pl.BlockSpec(memory_space=pl.ANY),
+        out_shape=jax.ShapeDtypeStruct(held.shape, held.dtype),
+        scratch_shapes=[pltpu.SemaphoreType.DMA((steps,))],
+        cost_estimate=pl.CostEstimate(
+            flops=1000 * held.size, bytes_accessed=4 * held.size, transcendentals=0
+        ),
+        compiler_params=pltpu.CompilerParams(vmem_limit_bytes=4 << 20),
+    )(held)
+
+
 def per_device(
     stream,
     norm_gain,
@@ -657,6 +1259,28 @@
     heads = decay_rate.shape[0]
     groups = lax.axis_size("tp") // heads
     weights = (query_weight, key_weight, value_weight, gate_weight)
+    rows, cols = stream.shape
+    if groups == 2 and heads == 16 and rows % 32 == 0 and rows <= 64 and cols % 256 == 0:
+        held, mine, rise = fused(
+            stream,
+            norm_gain,
+            weights,
+            write_weight,
+            decay_weight,
+            decay_rate,
+            head_gain,
+            out_weight,
+            state,
+            groups,
+        )
+        span = heads // 2
+        pairs = [
+            (i, i + span * (1 - 2 * (i // span % 2))) for i in range(lax.axis_size("tp"))
+        ]
+        arrived = lax.ppermute(rise, "tp", pairs)
+        updated = store(held)
+        result = stream.astype(jnp.float32) + mine + arrived.astype(jnp.float32)
+        return (result.astype(stream.dtype), updated)
     packed = project(
         stream, norm_gain, weights, write_weight, decay_weight, decay_rate, heads, groups
     )

time: 72.2 us -> 46 us (0.64)
  Pallas kernels: 69.8 us -> 44.4 us
  local copies, waits for them, and re-layouts: 1.57 us -> 0.01 us
    pallas_call x3 -> x2, Pallas kernels: 69.8 us -> 44.4 us  [the longest x1 38.5 us: fused(): pl.pallas_call(functools.partial(fused_kernel, heads, groups), in_specs=[...]
    unnamed x1 -> x2, local copies, waits for them, and re-layouts: 1.57 us -> 0.01 us
  transfers between devices with their start and end apart: 0 -> 1, of which waited for: 0 -> 0; matrix products, arithmetic and copies ran while one was open for 0% -> 0% of each run, Pallas kernels for 0% -> 13%
where the time goes in v2:
time: 46 us; the launch traced here: 45.9 us
  Pallas kernels  44.4 us (97%)
  other arithmetic  0.7 us (2%)
  between operations  0.68 us (1%)
    pallas_call x1, Pallas kernels, fused(): pl.pallas_call(functools.partial(fused_kernel, heads, groups), in_specs=[...  38.5 us
    pallas_call x1, Pallas kernels, store(): pl.pallas_call(store_kernel, in_specs=[VMEM], out_specs=pl.BlockSpec(memo...  5.92 us
  transfers between devices with their start and end apart: 1, of which 0 were waited for; matrix products, arithmetic and copies ran while one was open for 0% of the time, Pallas kernels for 13%

profile of v2, /device:TPU:0, one launch (start us, length us, event | category | flops | bytes accessed | tf_op | source)
XLA Modules:
  0.0 45.9 jit_solution(1763617122574237160)
XLA Ops:
  0.6 38.5 %shard_map.131 = (f32[256,128,128]{2,1,0:T(8,128)S(1)}, f32[32,2048]{1,0:T(8,128)S(1)}, bf16[32,2048]{1,0:T(8,128)(2,1)S(1)}) custom-call(bf16[32,2048]{1,0:T(8,128)(2,1)} %stream_hbm.1, bf16[32,128]{1,0:T(8,128)(2,1)} %bitcast.7, bf16[2048,128]{1,0:T(8,128)(2,1)} %query_w.1, bf16[2048,128]{1,0:T(8,128)(2,1)} %key_w.1, bf16[2048,128]{1,0:T(8,128)(2,1)} %value_w.1, ...), custom_call_target="tpu_custom_call" | custom-call | tf_op jit(solution)/shard_map/pallas_call | solution.py:1158
  39.1 0.1 collective-permute-start
  39.2 0.0 copy-start
  39.2 5.9 %shard_map.132 = f32[256,128,128]{2,1,0:T(8,128)} custom-call(f32[256,128,128]{2,1,0:T(8,128)S(1)} %get-tuple-element.7.held), custom_call_target="tpu_custom_call" | custom-call | flops 4194304000 | bytes 16777216 | tf_op jit(solution)/shard_map/pallas_call | solution.py:1232
  45.2 0.0 collective-permute-done
  45.2 0.0 copy-done
  45.2 0.7 %add_convert_fusion = bf16[32,2048]{1,0:T(8,128)(2,1)} fusion(bf16[32,2048]{1,0:T(8,128)(2,1)S(1)} %collective-permute-done, f32[32,2048]{1,0:T(8,128)S(1)} %get-tuple-element.5, bf16[32,2048]{1,0:T(8,128)(2,1)S(1)} %copy-done), kind=kLoop, calls=%fused_computation | loop fusion | flops 327680 | bytes 655360 | tf_op jit(solution)/shard_map/convert_element_type | solution.py:1283
Async XLA Ops:
  39.1 6.0 %collective-permute-start = (bf16[32,2048]{1,0:T(8,128)(2,1)S(1)}, bf16[32,2048]{1,0:T(8,128)(2,1)S(1)}, u32[]{:S(2)}, u32[]{:S(2)}) collective-permute-start(bf16[32,2048]{1,0:T(8,128)(2,1)S(1)} %get-tuple-element.6), channel_id=1, source_target_pairs={{0,8},{1,9},{2,10},{3,11},{4,12},{5,13},{6,14},{7,15},{8,0},{9,1},... | collective-permute-start | bytes 393224 | tf_op jit(solution)/shard_map/ppermute | solution.py:1280
  39.2 6.0 %copy-start = (bf16[32,2048]{1,0:T(8,128)(2,1)S(1)}, bf16[32,2048]{1,0:T(8,128)(2,1)}, u32[]{:S(2)}) copy-start(bf16[32,2048]{1,0:T(8,128)(2,1)} %stream_hbm.1) | copy-start | bytes 393220

commit v3 on v2

--- a/solution.py
+++ b/solution.py
@@ -11,6 +11,7 @@
 MESH = pl.DeviceIdType.MESH
 VMEM = pl.BlockSpec(memory_space=pltpu.VMEM)
 SMALL = 16
+TINY = 8
 
 
 def flip(me, bits):
@@ -669,6 +670,8 @@
     gathered,
     weights,
     side_w,
+    wide_side,
+    side_rows,
     gain_row,
     gains,
     four_w,
@@ -761,19 +764,23 @@
             out_w.at[spot, :],
             four_w.at[spot, 2 * size : 3 * size],
             pair_sems.at[3],
-            pair_sems.at[4 + h],
+            pair_sems.at[4 + i],
             neighbours[h],
         )
 
-    def passed_w(h, n=1):
-        spot = slice(h * wide_half, (h + n) * wide_half)
+    def passed_w(h, i):
+        spot = slice(h * wide_half + i * tall, h * wide_half + (i + 1) * tall)
         return remote(
             four_w.at[spot, 2 * size : 3 * size],
             four_w.at[spot, 3 * size : 4 * size],
             pair_sems.at[2],
-            pair_sems.at[6],
+            pair_sems.at[4 + pieces],
             sibling,
         )
+
+    def far_w(rows_of):
+        target = four_w.at[0:rows_of, 2 * size : 3 * size]
+        return target, target
 
     def fetch(c):
         spot = pl.ds(pl.multiple_of(c * chip_rows, chip_rows), chip_rows)
@@ -839,8 +846,11 @@
     tiles = cols // 128
     for i in range(tiles):
         gain_row[:, i * 128 : (i + 1) * 128] = gains[pl.ds(group * tiles + i, 1), :]
+    side_done.wait()
+    wide_side[...] = side_w[...].astype(jnp.float32)
+    for i in range(2):
+        side_rows[i : i + 1, :] = wide_side[pl.ds(i * heads + place, 1), :]
     weights_done.wait()
-    side_done.wait()
     for c in range(flats):
         fetch(chip_of(c)).start()
     own_w.start()
@@ -849,12 +859,9 @@
         x = gathered[pl.ds(pl.multiple_of(begin, chip_rows), high), :].astype(jnp.float32)
         gained = (x * gain_row[...]).astype(jnp.bfloat16)
         product = jnp.dot(gained, weights[...], preferred_element_type=jnp.float32)
-        pre = lax.dot_general(
-            gained, side_w[...], (((1,), (1,)), ((), ())), preferred_element_type=jnp.float32
-        )
-        spot = lax.broadcasted_iota(jnp.int32, pre.shape, 1)
-        write = jnp.sum(jnp.where(spot == place, pre, 0.0), axis=1, keepdims=True)
-        decay = jnp.sum(jnp.where(spot == place + heads, pre, 0.0), axis=1, keepdims=True)
+        exact = gained.astype(jnp.float32)
+        write = jnp.sum(exact * side_rows[0:1, :], axis=1, keepdims=True)
+        decay = jnp.sum(exact * side_rows[1:2, :], axis=1, keepdims=True)
         squares = jnp.sum(x * x, axis=1, keepdims=True)
         lane = lax.broadcasted_iota(jnp.int32, (high, 128), 1)
         side = jnp.where(
@@ -872,16 +879,20 @@
             small_sent.at[c], small_received.at[c], send_sems.at[3], small_recv.at[c], partner
         )
 
-    def project_away(c, raised):
+    def project_away(c, raised, send=True):
         from_sibling(c, raised)
         product, side = project(away_begin + chip_of(c) * chip_rows, chip_rows)
         sent[c] = product.astype(jnp.bfloat16)
-        main_copy(c).start()
         if chip_rows < 128:
             side = jnp.concatenate(
                 [side, jnp.zeros((128 - chip_rows, 128), jnp.float32)], axis=0
             )
-        small_sent[c] = side.T[0:SMALL].astype(jnp.bfloat16)
+        small_sent[c] = side.T[0:TINY].astype(jnp.bfloat16)
+        if send:
+            send_away(c)
+
+    def send_away(c):
+        main_copy(c).start()
         small_copy(c).start()
 
     def project_here(j, raised):
@@ -914,7 +925,7 @@
         whole = pl.ds(pl.multiple_of(begin, chip_rows), chip_rows)
         total = partial[whole, :] + received[c].astype(jnp.float32)
         flat = small_received[c].astype(jnp.float32)
-        flat = jnp.concatenate([flat, jnp.zeros((128 - SMALL, flat.shape[1]), jnp.float32)], axis=0)
+        flat = jnp.concatenate([flat, jnp.zeros((128 - TINY, flat.shape[1]), jnp.float32)], axis=0)
         side = partial_side[whole, :] + flat.T[0:chip_rows]
         scale = lax.rsqrt(side[:, 2:3] / (cols * groups) + EPS)
         projected = rounded(total * scale)
@@ -996,47 +1007,52 @@
 
         lax.fori_loop(0, chip_rows // count, body, 0)
 
-    def hop(phase, h):
+    def hop(phase, h, k):
         return remote(
-            hop_out.at[phase, h],
-            hop_in.at[phase, h],
+            hop_out.at[phase, h, k],
+            hop_in.at[phase, h, k],
             send_sems.at[5],
-            hop_recv.at[phase, h],
+            hop_recv.at[phase, h, k],
             neighbours[1 - h],
         )
 
+    slim = wide_half // 2
+
     def expand(phase):
-        for h in range(2):
-            span = slice(h * wide_half, (h + 1) * wide_half)
-            lefts = left[h, phase]
-            if h:
-                upper_rows = jnp.concatenate(
-                    [left[0, phase, 0:rows, 0 : 2 * size], lefts[0:rows, 2 * size :]], axis=1
+        lefts = [left[0, phase], left[1, phase]]
+        upper_rows = jnp.concatenate(
+            [lefts[0][0:rows, 0 : 2 * size], lefts[1][0:rows, 2 * size :]], axis=1
+        )
+        lefts[1] = jnp.concatenate([upper_rows, lefts[1][rows:]], axis=0)
+        for k in range(2):
+            for h in range(2):
+                begin = h * wide_half + k * slim
+                span = slice(begin, begin + slim)
+                product = lax.dot_general(
+                    lefts[h],
+                    four_w[span, :],
+                    (((1,), (1,)), ((), ())),
+                    preferred_element_type=jnp.float32,
                 )
-                lefts = jnp.concatenate([upper_rows, lefts[rows:]], axis=0)
-            product = lax.dot_general(
-                lefts,
-                four_w[span, :],
-                (((1,), (1,)), ((), ())),
-                preferred_element_type=jnp.float32,
-            )
-            hop_out[phase, h] = product[rows:].astype(jnp.bfloat16)
-            hop(phase, h).start()
-            acc[phase, :, span] = product[0:rows]
+                hop_out[phase, h, k] = product[rows:].astype(jnp.bfloat16)
+                hop(phase, h, k).start()
+                acc[phase, :, span] = product[0:rows]
 
     def settle(phase):
-        for q in range(2):
-            span = slice(q * wide_half, (q + 1) * wide_half)
-            hop(phase, q).wait_recv()
-            total = acc[phase, :, span] + hop_in[phase, q].astype(jnp.float32)
-
-            @pl.when(keep == phase)
-            def _():
-                mine_out[:, span] = total
-
-            @pl.when(keep != phase)
-            def _():
-                rise_out[:, span] = total.astype(jnp.bfloat16)
+        for k in range(2):
+            for h in range(2):
+                begin = h * wide_half + k * slim
+                span = slice(begin, begin + slim)
+                hop(phase, h, k).wait_recv()
+                total = acc[phase, :, span] + hop_in[phase, h, k].astype(jnp.float32)
+
+                @pl.when(keep == phase)
+                def _():
+                    mine_out[:, span] = total
+
+                @pl.when(keep != phase)
+                def _():
+                    rise_out[:, span] = total.astype(jnp.bfloat16)
 
     def gated_bytes(h, phase):
         blocks = (6, 8) if h == 0 else (5, 6)
@@ -1047,8 +1063,8 @@
             target = gated_bytes(h, phase)
             remote(target, target, send_sems.at[4], gated_recv.at[h, phase], sibling).wait_recv()
 
-    def relays(masks):
-        for q in range(2):
+    def relays(masks, halves=(0, 1)):
+        for q in halves:
             for p, mask in masks:
                 relay(p, q, mask)
 
@@ -1057,20 +1073,20 @@
             for h in range(2):
                 beside_w(h, i).start()
 
-    def pass_weights(h):
-        beside_w(h, 0, pieces).wait_recv()
-        passed_w(h).start()
+    def pass_weights(i):
+        remote(*far_w(2 * tall), pair_sems.at[3], pair_sems.at[4 + i], sibling).wait_recv()
+        for h in range(2):
+            passed_w(h, i).start()
 
     def weights_ready():
         own_w.wait()
         sibling_w.wait_recv()
-        passed_w(0, 2).wait_recv()
+        remote(*far_w(cols), pair_sems.at[3], pair_sems.at[4 + pieces], sibling).wait_recv()
 
     def drain():
         sibling_w.wait_send()
-        passed_w(0, 2).wait_send()
-        for h in range(2):
-            beside_w(h, 0, pieces).wait_send()
+        for i in range(2, 4):
+            remote(*far_w(cols), pair_sems.at[i], pair_sems.at[4], sibling).wait_send()
         ici_rows = rows * (chips - 1)
         for i, ref in enumerate(
             (gathered.at[0:ici_rows, :], gathered.at[0 : rows * chips, :], sent, small_sent)
@@ -1080,18 +1096,17 @@
             for h in range(2):
                 target = gated_bytes(h, phase)
                 remote(target, target, send_sems.at[4], gated_recv.at[0, 0], sibling).wait_send()
-        remote(hop_out, hop_in, send_sems.at[5], hop_recv.at[0, 0], sibling).wait_send()
+        remote(hop_out, hop_in, send_sems.at[5], hop_recv.at[0, 0, 0], sibling).wait_send()
 
     @pl.when(outer == 1)
     def _():
         relays([(0, z), (1, z)])
         project_away(0, 1)
+        relays([(0, x + z), (1, y + z), (1, x + z), (0, y + z)])
         relays([(0, x), (1, y), (1, x), (0, y)])
-        send_beside(0, 1)
-        relays([(0, x + z), (1, y + z), (1, x + z), (0, y + z)])
+        send_beside(0, pieces)
         project_away(1, 1)
         project_away(2, 1)
-        send_beside(1, pieces)
         project_here(0, 0)
         relays([(0, x + y + z), (1, x + y + z)])
         project_away(3, 1)
@@ -1100,35 +1115,40 @@
 
     @pl.when(outer == 0)
     def _():
-        project_away(0, 0)
-        relays([(0, x), (1, y), (1, x), (0, y)])
+        project_away(0, 0, False)
+        relays([(0, x), (1, y), (1, x), (0, y)], (0,))
+        send_away(0)
+        relays([(0, x), (1, y), (1, x), (0, y)], (1,))
         project_away(1, 0)
         project_away(2, 0)
         relays([(0, z), (1, z)])
+        send_beside(0, 1)
         relays([(0, x + y), (1, x + y)])
         project_away(3, 0)
         relays([(0, x + z), (1, y + z), (1, x + z), (0, y + z)])
-        send_beside(0, pieces)
+        send_beside(1, pieces)
         project_here(0, 1)
         relays([(0, x + y + z), (1, x + y + z)])
         project_here(1, 1)
 
     recall(0)
     recall(1)
+    pass_weights(0)
     recall(2)
+    pass_weights(1)
+    pass_weights(2)
+    pass_weights(3)
     recall(3)
-    pass_weights(0)
-    pass_weights(1)
+    update(0)
     weights_ready()
     whole_left(0)
     expand(0)
-    update(0)
     update(1)
     whole_left(1)
     expand(1)
     update(2)
+    update(3)
     settle(0)
-    update(3)
     settle(1)
     drain()
 
@@ -1172,6 +1192,8 @@
             pltpu.VMEM((batch, cols), bf16),
             pltpu.VMEM((cols, 4 * size), bf16),
             pltpu.VMEM((2 * heads, cols), bf16),
+            pltpu.VMEM((2 * heads, cols), f32),
+            pltpu.VMEM((2, cols), f32),
             pltpu.VMEM((1, cols), f32),
             pltpu.VMEM((groups * cols // 128, 128), f32),
             pltpu.VMEM((cols, 4 * size), bf16),
@@ -1179,25 +1201,25 @@
             pltpu.VMEM((flats * chip_rows, 128), f32),
             pltpu.VMEM((flats, chip_rows, 4 * size), bf16),
             pltpu.VMEM((flats, chip_rows, 4 * size), bf16),
-            pltpu.VMEM((flats, SMALL, max(128, chip_rows)), bf16),
-            pltpu.VMEM((flats, SMALL, max(128, chip_rows)), bf16),
+            pltpu.VMEM((flats, TINY, max(128, chip_rows)), bf16),
+            pltpu.VMEM((flats, TINY, max(128, chip_rows)), bf16),
             pltpu.VMEM((flats, 3, chip_rows, size), f32),
             pltpu.VMEM((2, chip_rows, size), f32),
             pltpu.VMEM((flats, chip_rows, size), bf16),
             pltpu.VMEM((2, 2, 2 * rows, 4 * size), bf16),
             pltpu.VMEM((2, rows, cols), f32),
-            pltpu.VMEM((2, 2, rows, cols // 2), bf16),
-            pltpu.VMEM((2, 2, rows, cols // 2), bf16),
+            pltpu.VMEM((2, 2, 2, rows, cols // 4), bf16),
+            pltpu.VMEM((2, 2, 2, rows, cols // 4), bf16),
             dma((7,)),
             dma((flats,)),
-            dma((7,)),
+            dma((9,)),
             dma((6,)),
             dma((2, 2, chips - 1)),
             dma((chips,)),
             dma((flats,)),
             dma((flats,)),
             dma((2, 2)),
-            dma((2, 2)),
+            dma((2, 2, 2)),
         ],
         compiler_params=pltpu.CompilerParams(
             collective_id=2, has_side_effects=True, vmem_limit_bytes=43 << 20

time: 46 us -> 44.5 us (0.967)
  Pallas kernels: 44.4 us -> 41.4 us
  starting transfers between devices: 0.07 us -> 1.56 us
    pallas_call x1, Pallas kernels: 38.5 us -> 35.5 us  [fused(): pl.pallas_call(functools.partial(fused_kernel, heads, groups), in_specs=[...]
    ppermute x1, starting transfers between devices: 0.07 us -> 1.56 us  [per_device(): arrived = lax.ppermute(rise, 'tp', pairs)]
where the time goes in v3:
time: 44.5 us; the launch traced here: 44.3 us
  Pallas kernels  41.4 us (93%)
  starting transfers between devices  1.56 us (4%)
  other arithmetic  0.7 us (2%)
  between operations  0.67 us (2%)
    pallas_call x1, Pallas kernels, fused(): pl.pallas_call(functools.partial(fused_kernel, heads, groups), in_specs=[...  35.5 us
    pallas_call x1, Pallas kernels, store(): pl.pallas_call(store_kernel, in_specs=[VMEM], out_specs=pl.BlockSpec(memo...  5.92 us
    ppermute x1, starting transfers between devices, per_device(): arrived = lax.ppermute(rise, 'tp', pairs)  1.56 us
  transfers between devices with their start and end apart: 1, of which 0 were waited for; matrix products, arithmetic and copies ran while one was open for 0% of the time, Pallas kernels for 13%

profile of v3, /device:TPU:0, one launch (start us, length us, event | category | flops | bytes accessed | tf_op | source)
XLA Modules:
  0.0 44.3 jit_solution(16485748722464358380)
XLA Ops:
  0.6 35.5 %shard_map.131 = (f32[256,128,128]{2,1,0:T(8,128)S(1)}, f32[32,2048]{1,0:T(8,128)S(1)}, bf16[32,2048]{1,0:T(8,128)(2,1)S(1)}) custom-call(bf16[32,2048]{1,0:T(8,128)(2,1)} %stream_hbm.1, bf16[32,128]{1,0:T(8,128)(2,1)} %bitcast.7, bf16[2048,128]{1,0:T(8,128)(2,1)} %query_w.1, bf16[2048,128]{1,0:T(8,128)(2,1)} %key_w.1, bf16[2048,128]{1,0:T(8,128)(2,1)} %value_w.1, ...), custom_call_target="tpu_custom_call" | custom-call | tf_op jit(solution)/shard_map/pallas_call | solution.py:1178
  36.1 1.6 %collective-permute-start = (bf16[32,2048]{1,0:T(8,128)(2,1)S(1)}, bf16[32,2048]{1,0:T(8,128)(2,1)S(1)}, u32[]{:S(2)}, u32[]{:S(2)}) collective-permute-start(bf16[32,2048]{1,0:T(8,128)(2,1)S(1)} %get-tuple-element.6), channel_id=1, source_target_pairs={{0,8},{1,9},{2,10},{3,11},{4,12},{5,13},{6,14},{7,15},{8,0},{9,1},... | collective-permute-start | bytes 393224 | tf_op jit(solution)/shard_map/ppermute | solution.py:1302
  37.7 0.0 copy-start
  37.7 5.9 %shard_map.132 = f32[256,128,128]{2,1,0:T(8,128)} custom-call(f32[256,128,128]{2,1,0:T(8,128)S(1)} %get-tuple-element.7.held), custom_call_target="tpu_custom_call" | custom-call | flops 4194304000 | bytes 16777216 | tf_op jit(solution)/shard_map/pallas_call | solution.py:1254
  43.6 0.0 collective-permute-done
  43.6 0.0 copy-done
  43.6 0.7 %add_convert_fusion = bf16[32,2048]{1,0:T(8,128)(2,1)} fusion(bf16[32,2048]{1,0:T(8,128)(2,1)S(1)} %collective-permute-done, f32[32,2048]{1,0:T(8,128)S(1)} %get-tuple-element.5, bf16[32,2048]{1,0:T(8,128)(2,1)S(1)} %copy-done), kind=kLoop, calls=%fused_computation | loop fusion | flops 327680 | bytes 655360 | tf_op jit(solution)/shard_map/convert_element_type | solution.py:1305
Async XLA Ops:
  36.1 7.5 %collective-permute-start = (bf16[32,2048]{1,0:T(8,128)(2,1)S(1)}, bf16[32,2048]{1,0:T(8,128)(2,1)S(1)}, u32[]{:S(2)}, u32[]{:S(2)}) collective-permute-start(bf16[32,2048]{1,0:T(8,128)(2,1)S(1)} %get-tuple-element.6), channel_id=1, source_target_pairs={{0,8},{1,9},{2,10},{3,11},{4,12},{5,13},{6,14},{7,15},{8,0},{9,1},... | collective-permute-start | bytes 393224 | tf_op jit(solution)/shard_map/ppermute | solution.py:1302
  37.7 5.9 %copy-start = (bf16[32,2048]{1,0:T(8,128)(2,1)S(1)}, bf16[32,2048]{1,0:T(8,128)(2,1)}, u32[]{:S(2)}) copy-start(bf16[32,2048]{1,0:T(8,128)(2,1)} %stream_hbm.1) | copy-start | bytes 393220

commit v4 on v3

--- a/solution.py
+++ b/solution.py
@@ -645,6 +645,32 @@
     return tuple(bit for bit in range(1, dims + 1) if mask >> (bit - 1) & 1)
 
 
+def renew(kept, read, write):
+    count = 16
+    _, total, size = kept.shape
+    spots = lax.broadcasted_iota(jnp.int32, (3 * count, size), 0) % count
+
+    def body(i, carry):
+        near = pl.ds(pl.multiple_of(i * count, count), count)
+        key_high, key_low = split(kept[0, near, :])
+        change_high, change_low = split(kept[1, near, :])
+        factor = kept[2, near, :]
+        keys = jnp.concatenate([key_high, key_low, key_high], axis=0)
+        keys = jnp.concatenate([keys, jnp.zeros((size - 3 * count, size), keys.dtype)], axis=0)
+        keys = keys.astype(jnp.float32).T.astype(jnp.bfloat16)[:, 0 : 3 * count]
+        changes = jnp.concatenate([change_high, change_high, change_low], axis=0)
+        wide = jnp.concatenate(
+            [jnp.where(spots == b, changes, jnp.zeros_like(changes)) for b in range(count)], axis=1
+        )
+        outer = jnp.dot(keys, wide, preferred_element_type=jnp.float32)
+        for b in range(count):
+            spot = i * count + b
+            write(spot, factor[b : b + 1, :] * read(spot) + outer[:, b * size : (b + 1) * size])
+        return carry
+
+    lax.fori_loop(0, total // count, body, 0)
+
+
 def fused_kernel(
     heads,
     groups,
@@ -663,6 +689,7 @@
     held,
     mine_out,
     rise_out,
+    late,
     stream_ref,
     gain_ref,
     rate_ref,
@@ -979,33 +1006,18 @@
                     left[h, 0, span, 0:size] = gated[
                         c, pl.ds(pl.multiple_of(core * rows, rows), rows), :
                     ]
-        packed[c, 0] = key
-        packed[c, 1] = change
-        packed[c, 2] = factor
+        kept = packed.at[c] if c < flats - 1 else late
+        kept[0] = key
+        kept[1] = change
+        kept[2] = factor
 
     def update(c):
         begin = chip_of(c) * chip_rows
-        spots = marks(3)
-
-        def body(i, carry):
-            near = pl.ds(pl.multiple_of(i * count, count), count)
-            key_high, key_low = split(packed[c, 0, near, :])
-            change_high, change_low = split(packed[c, 1, near, :])
-            factor = packed[c, 2, near, :]
-            keys = jnp.concatenate([key_high, key_low, key_high], axis=0)
-            keys = jnp.concatenate([keys, jnp.zeros((size - 3 * count, size), keys.dtype)], axis=0)
-            keys = keys.astype(jnp.float32).T.astype(jnp.bfloat16)[:, 0 : 3 * count]
-            wide = diagonal(jnp.concatenate([change_high, change_high, change_low], axis=0), spots)
-            outer_product = jnp.dot(keys, wide, preferred_element_type=jnp.float32)
-            for b in range(count):
-                spot = begin + i * count + b
-                held[spot] = (
-                    factor[b : b + 1, :] * held[spot]
-                    + outer_product[:, b * size : (b + 1) * size]
-                )
-            return carry
-
-        lax.fori_loop(0, chip_rows // count, body, 0)
+
+        def write(i, value):
+            held[begin + i] = value
+
+        renew(packed.at[c], lambda i: held[begin + i], write)
 
     def hop(phase, h, k):
         return remote(
@@ -1143,11 +1155,10 @@
     weights_ready()
     whole_left(0)
     expand(0)
-    update(1)
     whole_left(1)
     expand(1)
+    update(1)
     update(2)
-    update(3)
     settle(0)
     settle(1)
     drain()
@@ -1178,11 +1189,12 @@
     return pl.pallas_call(
         functools.partial(fused_kernel, heads, groups),
         in_specs=[anywhere] * 12,
-        out_specs=[VMEM] * 3,
+        out_specs=[VMEM] * 4,
         out_shape=[
             pltpu.VMEM(state.shape, state.dtype),
             pltpu.VMEM(stream.shape, f32),
             pltpu.VMEM(stream.shape, bf16),
+            pltpu.VMEM((3, chip_rows, size), f32),
         ],
         scratch_shapes=[
             pltpu.VMEM(stream.shape, stream.dtype),
@@ -1237,31 +1249,47 @@
     )
 
 
-def store_kernel(held, new_ref, sems):
-    steps = sems.shape[0]
-    count = held.shape[0] // steps
-    copies = []
-    for step in range(steps):
-        spot = slice(step * count, (step + 1) * count)
-        copies.append(pltpu.make_async_copy(held.at[spot], new_ref.at[spot], sems.at[step]))
-        copies[-1].start()
-    for copy in copies:
-        copy.wait()
-
-
-def store(held):
-    steps = min(8, held.shape[0])
+def store_kernel(heads, held, late, new_ref, fresh, sems):
+    place = lax.axis_index("tp") % heads
+    count = late.shape[1]
+    chunks = held.shape[0] // count
+    last = chunks - 1 - place // 2 % chunks
+
+    def copy(i, source):
+        spot = pl.ds(pl.multiple_of((last + i) % chunks * count, count), count)
+        origin = held.at[spot] if source is None else source
+        return pltpu.make_async_copy(origin, new_ref.at[spot], sems.at[i])
+
+    for i in range(1, chunks):
+        copy(i, None).start()
+
+    def write(i, value):
+        fresh[i] = value
+
+    renew(late, lambda i: held[last * count + i], write)
+    copy(0, fresh).start()
+    for i in range(1, chunks):
+        copy(i, None).wait()
+    copy(0, fresh).wait()
+
+
+def store(held, late, heads):
+    total, size, _ = held.shape
+    count = late.shape[1]
     return pl.pallas_call(
-        store_kernel,
-        in_specs=[VMEM],
+        functools.partial(store_kernel, heads),
+        in_specs=[VMEM] * 2,
         out_specs=pl.BlockSpec(memory_space=pl.ANY),
         out_shape=jax.ShapeDtypeStruct(held.shape, held.dtype),
-        scratch_shapes=[pltpu.SemaphoreType.DMA((steps,))],
+        scratch_shapes=[
+            pltpu.VMEM((count, size, size), held.dtype),
+            pltpu.SemaphoreType.DMA((total // count,)),
+        ],
         cost_estimate=pl.CostEstimate(
             flops=1000 * held.size, bytes_accessed=4 * held.size, transcendentals=0
         ),
-        compiler_params=pltpu.CompilerParams(vmem_limit_bytes=4 << 20),
-    )(held)
+        compiler_params=pltpu.CompilerParams(vmem_limit_bytes=10 << 20),
+    )(held, late)
 
 
 def per_device(
@@ -1283,7 +1311,7 @@
     weights = (query_weight, key_weight, value_weight, gate_weight)
     rows, cols = stream.shape
     if groups == 2 and heads == 16 and rows % 32 == 0 and rows <= 64 and cols % 256 == 0:
-        held, mine, rise = fused(
+        held, mine, rise, late = fused(
             stream,
             norm_gain,
             weights,
@@ -1300,7 +1328,7 @@
             (i, i + span * (1 - 2 * (i // span % 2))) for i in range(lax.axis_size("tp"))
         ]
         arrived = lax.ppermute(rise, "tp", pairs)
-        updated = store(held)
+        updated = store(held, late, heads)
         result = stream.astype(jnp.float32) + mine + arrived.astype(jnp.float32)
         return (result.astype(stream.dtype), updated)
     packed = project(

time: 44.5 us -> 44.2 us (level)
  Pallas kernels: 41.4 us -> 40.3 us
  starting transfers between devices: 1.56 us -> 2.34 us
    pallas_call x1, Pallas kernels: 35.5 us -> 34.3 us  [fused(): pl.pallas_call(functools.partial(fused_kernel, heads, groups), in_specs=[...]
    ppermute x1, starting transfers between devices: 1.56 us -> 2.34 us  [per_device(): arrived = lax.ppermute(rise, 'tp', pairs)]
  transfers between devices with their start and end apart: 1 -> 1, of which waited for: 0 -> 0; matrix products, arithmetic and copies ran while one was open for 0% -> 0% of each run, Pallas kernels for 13% -> 14%
where the time goes in v4:
time: 44.2 us; the launch traced here: 44 us
  Pallas kernels  40.3 us (91%)
  starting transfers between devices  2.34 us (5%)
  other arithmetic  0.7 us (2%)
  between operations  0.67 us (2%)
    pallas_call x1, Pallas kernels, fused(): pl.pallas_call(functools.partial(fused_kernel, heads, groups), in_specs=[...  34.3 us
    pallas_call x1, Pallas kernels, store(): pl.pallas_call(functools.partial(store_kernel, heads), in_specs=[VMEM] *...  5.95 us
    ppermute x1, starting transfers between devices, per_device(): arrived = lax.ppermute(rise, 'tp', pairs)  2.34 us
  transfers between devices with their start and end apart: 1, of which 0 were waited for; matrix products, arithmetic and copies ran while one was open for 0% of the time, Pallas kernels for 14%

profile of v4, /device:TPU:0, one launch (start us, length us, event | category | flops | bytes accessed | tf_op | source)
XLA Modules:
  0.0 44.0 jit_solution(16394795251567254763)
XLA Ops:
  0.6 34.3 %shard_map.131 = (f32[256,128,128]{2,1,0:T(8,128)S(1)}, f32[32,2048]{1,0:T(8,128)S(1)}, bf16[32,2048]{1,0:T(8,128)(2,1)S(1)}, f32[3,64,128]{2,1,0:T(8,128)S(1)}) custom-call(bf16[32,2048]{1,0:T(8,128)(2,1)} %stream_hbm.1, bf16[32,128]{1,0:T(8,128)(2,1)} %bitcast.7, bf16[2048,128]{1,0:T(8,128)(2,1)} %query_w.1, bf16[2048,128]{1,0:T(8,128)(2,1)} %key_w.1, ...), custom_call_target="tpu_custom_call" | custom-call | tf_op jit(solution)/shard_map/pallas_call | solution.py:1189
  35.0 2.3 %collective-permute-start = (bf16[32,2048]{1,0:T(8,128)(2,1)S(1)}, bf16[32,2048]{1,0:T(8,128)(2,1)S(1)}, u32[]{:S(2)}, u32[]{:S(2)}) collective-permute-start(bf16[32,2048]{1,0:T(8,128)(2,1)S(1)} %get-tuple-element.7), channel_id=1, source_target_pairs={{0,8},{1,9},{2,10},{3,11},{4,12},{5,13},{6,14},{7,15},{8,0},{9,1},... | collective-permute-start | bytes 393224 | tf_op jit(solution)/shard_map/ppermute | solution.py:1330
  37.3 0.0 copy-start
  37.3 6.0 %shard_map.132 = f32[256,128,128]{2,1,0:T(8,128)} custom-call(f32[256,128,128]{2,1,0:T(8,128)S(1)} %get-tuple-element.8.held, f32[3,64,128]{2,1,0:T(8,128)S(1)} %get-tuple-element.9.late), custom_call_target="tpu_custom_call" | custom-call | flops 4194304000 | bytes 16777216 | tf_op jit(solution)/shard_map/pallas_call | solution.py:1279
  43.3 0.0 collective-permute-done
  43.3 0.0 copy-done
  43.3 0.7 %add_convert_fusion = bf16[32,2048]{1,0:T(8,128)(2,1)} fusion(bf16[32,2048]{1,0:T(8,128)(2,1)S(1)} %collective-permute-done, f32[32,2048]{1,0:T(8,128)S(1)} %get-tuple-element.6, bf16[32,2048]{1,0:T(8,128)(2,1)S(1)} %copy-done), kind=kLoop, calls=%fused_computation | loop fusion | flops 327680 | bytes 655360 | tf_op jit(solution)/shard_map/convert_element_type | solution.py:1333
Async XLA Ops:
  35.0 8.3 %collective-permute-start = (bf16[32,2048]{1,0:T(8,128)(2,1)S(1)}, bf16[32,2048]{1,0:T(8,128)(2,1)S(1)}, u32[]{:S(2)}, u32[]{:S(2)}) collective-permute-start(bf16[32,2048]{1,0:T(8,128)(2,1)S(1)} %get-tuple-element.7), channel_id=1, source_target_pairs={{0,8},{1,9},{2,10},{3,11},{4,12},{5,13},{6,14},{7,15},{8,0},{9,1},... | collective-permute-start | bytes 393224 | tf_op jit(solution)/shard_map/ppermute | solution.py:1330
  37.3 6.0 %copy-start = (bf16[32,2048]{1,0:T(8,128)(2,1)S(1)}, bf16[32,2048]{1,0:T(8,128)(2,1)}, u32[]{:S(2)}) copy-start(bf16[32,2048]{1,0:T(8,128)(2,1)} %stream_hbm.1) | copy-start | bytes 393220
